TPU v7x, 1024 devices: a whole 4x4x32 slice. The times are simulated.
1024 devices in a mesh: pp: 32 (over z), fs: 4 (over y), tp: 8 (over x, core).
Axes of the slice: x: 4, y: 4, z: 32, core: 2. Of those that a mesh axis runs over, the one named last changes fastest.
Arguments:
- tokens_in: bfloat16 [32, 32, 8, 2048], P('pp', ('fs', 'tp')), may hold values from -6 to 6
- weight_in: bfloat16 [32, 2048, 512], P('pp'), may hold values from -0.125 to 0.125
- conv_taps: float32 [32, 4, 512], P('pp'), may hold values from -3 to 3
- conv_bias: float32 [32, 512], P('pp'), may hold values from -2 to 2
- gate_rate: bfloat16 [32, 8, 64, 64], P('pp'), may hold values from -0.75 to 0.75
- bias_rate: float32 [32, 512], P('pp'), may hold values from -3 to 3
- gate_input: bfloat16 [32, 8, 64, 64], P('pp'), may hold values from -0.75 to 0.75
- bias_input: float32 [32, 512], P('pp'), may hold values from -3 to 3
- decay_param: float32 [32, 512], P('pp'), may hold values from 3.5 to 7.5
- weight_out: bfloat16 [32, 512, 2048], P('pp'), may hold values from -0.5 to 0.5
- norm_gain: float32 [32, 2048], P('pp'), may hold values from 0.1 to 1.9
- norm_shift: float32 [32, 2048], P('pp'), may hold values from -2 to 2
Outputs:
- tokens_out: bfloat16 [32, 32, 8, 2048], P('pp', ('fs', 'tp'))
All inputs are finite; a program needn't handle non-finite values.
Results may differ from a plain program's by a relative error of at most 0.022.
Values may be sent and summed in bfloat16 or wider, within the bound.
No kernel may reach another device: no remote copies, remote signals or barrier semaphores. Data moves between devices by JAX's collectives and lax.ppermute only.
A program may use at most 128 MiB of HBM per device.

v0:
```python
import jax
import jax.numpy as jnp
from jax import lax
from jax.sharding import PartitionSpec as P

decay_scale = 8.0
norm_eps = 1e-05


def passed_along(x, axis, by):
    length = lax.axis_size(axis)
    pairs = [(i, i + by) for i in range(length) if 0 <= i + by < length]
    return lax.ppermute(x, axis, pairs)


def combine_steps(earlier, later):
    return (earlier[0] * later[0], later[0] * earlier[1] + later[1])


def recurrence(
    projected, conv_taps, conv_bias, gate_rate, bias_rate, gate_input, bias_input, decay_param
):
    seq_count, length, channels = projected.shape
    tap_count = conv_taps.shape[0]
    padded = jnp.pad(projected.astype(jnp.float32), ((0, 0), (tap_count - 1, 0), (0, 0)))
    convolved = conv_bias + padded[:, 0:length] * conv_taps[0]
    for tap_index in range(1, tap_count):
        convolved = convolved + padded[:, tap_index : tap_index + length] * conv_taps[tap_index]
    convolved = convolved.astype(jnp.bfloat16)
    blocks = gate_rate.shape[0]
    block_width = gate_rate.shape[1]
    grouped = convolved.reshape(seq_count, length, blocks, block_width)
    rate_pre = jnp.einsum("bsnc,ncd->bsnd", grouped, gate_rate, preferred_element_type=jnp.float32)
    input_pre = jnp.einsum(
        "bsnc,ncd->bsnd", grouped, gate_input, preferred_element_type=jnp.float32
    )
    rate_gate = jax.nn.sigmoid(rate_pre.reshape(seq_count, length, channels) + bias_rate)
    input_gate = jax.nn.sigmoid(input_pre.reshape(seq_count, length, channels) + bias_input)
    log_decay = -decay_scale * rate_gate * jax.nn.softplus(-decay_param)
    scale_in = jnp.sqrt(-jnp.expm1(2.0 * log_decay))
    driven = scale_in * input_gate * convolved.astype(jnp.float32)
    decay_now = jnp.exp(log_decay)
    unused, hidden = lax.associative_scan(combine_steps, (decay_now, driven), axis=1)
    return hidden.astype(jnp.bfloat16)


def shards(
    tokens_in,
    weight_in,
    conv_taps,
    conv_bias,
    gate_rate,
    bias_rate,
    gate_input,
    bias_input,
    decay_param,
    weight_out,
    norm_gain,
    norm_shift,
):
    section_count = lax.axis_size("pp")
    section_index = lax.axis_index("pp")
    micro_count = section_count // 2
    length = tokens_in.shape[2]
    model_width = tokens_in.shape[3]
    w_project = weight_in[0]
    w_back = weight_out[0]
    lru_width = w_project.shape[1]

    def section_apply(entry_rows, is_valid):
        pair_count = entry_rows.shape[0]
        flat_rows = entry_rows.reshape(pair_count * length, model_width)

        def run_section():
            projected = jnp.dot(flat_rows, w_project, preferred_element_type=jnp.float32).astype(
                jnp.bfloat16
            )
            mixed_out = recurrence(
                projected.reshape(pair_count, length, lru_width),
                conv_taps[0],
                conv_bias[0],
                gate_rate[0],
                bias_rate[0],
                gate_input[0],
                bias_input[0],
                decay_param[0],
            )
            summed = flat_rows.astype(jnp.float32) + jnp.dot(
                mixed_out.reshape(pair_count * length, lru_width),
                w_back,
                preferred_element_type=jnp.float32,
            )
            mean_value = jnp.mean(summed, axis=-1, keepdims=True)
            centered = summed - mean_value
            variance = jnp.mean(centered * centered, axis=-1, keepdims=True)
            normed = centered * lax.rsqrt(variance + norm_eps) * norm_gain[0] + norm_shift[0]
            return normed.astype(jnp.bfloat16).reshape(pair_count, length, model_width)

        return lax.cond(
            is_valid,
            run_section,
            lambda: jnp.zeros((pair_count, length, model_width), jnp.bfloat16),
        )

    def advance(step_index, moving, out_buffer, first_input):
        entry_rows = jnp.where(section_index == 0, first_input, moving)
        offset = step_index - section_index
        is_valid = (offset >= 0) & (offset < micro_count)
        result = section_apply(entry_rows, is_valid)
        moving_next = passed_along(result, "pp", 1)
        out_slot = jnp.clip(step_index - (section_count - 1), 0, micro_count - 1).astype(jnp.int32)
        do_write = (section_index == section_count - 1) & (step_index >= section_count - 1)
        current = lax.dynamic_index_in_dim(out_buffer, out_slot, 0, keepdims=False)
        out_buffer = lax.dynamic_update_index_in_dim(
            out_buffer, jnp.where(do_write, result, current), out_slot, 0
        )
        return (moving_next, out_buffer)

    blank_rows = jnp.zeros((2, length, model_width), jnp.bfloat16)
    out_buffer = jnp.zeros((micro_count, 2, length, model_width), jnp.bfloat16)
    everyone = lax.all_gather(tokens_in, "pp", axis=0, tiled=True)

    def feed_turn(step_index, state_pair):
        first_input = lax.dynamic_slice_in_dim(everyone, 2 * step_index, 2, 0).reshape(
            2, length, model_width
        )
        return advance(step_index, state_pair[0], state_pair[1], first_input)

    moving, out_buffer = lax.fori_loop(0, micro_count, feed_turn, (blank_rows, out_buffer))

    def drain_turn(step_index, state_pair):
        return advance(step_index, state_pair[0], state_pair[1], state_pair[0])

    moving, out_buffer = lax.fori_loop(
        micro_count, micro_count + section_count - 1, drain_turn, (moving, out_buffer)
    )
    by_slot = out_buffer.reshape(section_count, length, model_width)
    arrived = lax.all_to_all(by_slot, "pp", split_axis=0, concat_axis=0, tiled=True)
    own_entry = arrived[section_count - 1 : section_count]
    return own_entry.reshape(1, 1, length, model_width)


def solution(mesh):
    placed = (
        P("pp", ("fs", "tp"), None, None),
        P("pp", None, None),
        P("pp", None, None),
        P("pp", None),
        P("pp", None, None, None),
        P("pp", None),
        P("pp", None, None, None),
        P("pp", None),
        P("pp", None),
        P("pp", None, None),
        P("pp", None),
        P("pp", None),
    )
    return jax.shard_map(
        shards,
        mesh=mesh,
        in_specs=placed,
        out_specs=P("pp", ("fs", "tp"), None, None),
        check_vma=False,
    )
```

profile of v0, /device:TPU:6, one launch (start us, length us, event | category | flops | bytes accessed | tf_op | source)
XLA Modules:
  0.0 886.7 jit_solution(971353123846458805)
XLA Ops:
  7.3 146.7 %all-gather.2.cloned.1.call-done = bf16[32,1,8,2048]{3,2,1,0:T(8,128)(2,1)} async-done(((bf16[1,1,8,2048]{3,2,1,0:T(8,128)(2,1)}), bf16[32,1,8,2048]{3,2,1,0:T(8,128)(2,1)}) %all-gather.2.cloned.1.call-update) | async-done | bytes 1048592 | tf_op jit(solution)/shard_map/all_gather | solution.py:121
  154.1 226.8 %while.36 = (s32[]{:T(128)}, bf16[2,8,2048]{2,1,0:T(8,128)(2,1)S(1)}, bf16[16,2,8,2048]{3,2,1,0:T(8,128)(2,1)S(1)}, s32[]{:T(128)}, pred[]{:T(512)}, /*index=5*/...) while((s32[]{:T(128)}, ...), condition=%wide.region_5.6_spmd, body=%wide.region_0.5_spmd.sunk | while | flops 70007832 | bytes 16224151 | solution.py:129
  154.1 8.0 conditional.4
  165.3 7.9 conditional.4
  179.4 7.9 conditional.4
  250.4 7.9 conditional.4
  264.5 7.9 conditional.4
  278.6 7.9 conditional.4
  335.0 7.9 conditional.4
  380.9 294.5 %while.37 = (s32[]{:T(128)}, bf16[2,8,2048]{2,1,0:T(8,128)(2,1)S(1)}, bf16[16,2,8,2048]{3,2,1,0:T(8,128)(2,1)S(1)}, s32[]{:T(128)}, f32[1,512]{1,0:T(1,128)}, /*...) while((s32[]{:T(128)}, ...), condition=%wide.region_11.12_spmd, body=%wide.region_6.11_spmd.sunk | while | flops 69942296 | bytes 16059688 | solution.py:134
  380.9 12.8 %collective-permute-start.1 = (bf16[2,8,2048]{2,1,0:T(8,128)(2,1)S(1)}, bf16[2,8,2048]{2,1,0:T(8,128)(2,1)S(1)}, u32[]{:S(2)}, u32[]{:S(2)}) collective-permute-start(bf16[2,8,2048]{2,1,0:T(8,128)(2,1)S(1)} %get-tuple-element.1520), channel_id=1, source_target_pairs={{0,32},{32,64},{64,96},{96,128},{128,160},{160,192},{192,224},{224... | collective-permute-start | bytes 196616 | tf_op jit(solution)/shard_map/while/body/eval_jaxpr/ppermute | solution.py:13
  403.0 13.0 %collective-permute-start.1 = (bf16[2,8,2048]{2,1,0:T(8,128)(2,1)S(1)}, bf16[2,8,2048]{2,1,0:T(8,128)(2,1)S(1)}, u32[]{:S(2)}, u32[]{:S(2)}) collective-permute-start(bf16[2,8,2048]{2,1,0:T(8,128)(2,1)S(1)} %get-tuple-element.1520), channel_id=1, source_target_pairs={{0,32},{32,64},{64,96},{96,128},{128,160},{160,192},{192,224},{224... | collective-permute-start | bytes 196616 | tf_op jit(solution)/shard_map/while/body/eval_jaxpr/ppermute | solution.py:13
  425.5 12.3 %collective-permute-start.1 = (bf16[2,8,2048]{2,1,0:T(8,128)(2,1)S(1)}, bf16[2,8,2048]{2,1,0:T(8,128)(2,1)S(1)}, u32[]{:S(2)}, u32[]{:S(2)}) collective-permute-start(bf16[2,8,2048]{2,1,0:T(8,128)(2,1)S(1)} %get-tuple-element.1520), channel_id=1, source_target_pairs={{0,32},{32,64},{64,96},{96,128},{128,160},{160,192},{192,224},{224... | collective-permute-start | bytes 196616 | tf_op jit(solution)/shard_map/while/body/eval_jaxpr/ppermute | solution.py:13
  447.1 12.8 %collective-permute-start.1 = (bf16[2,8,2048]{2,1,0:T(8,128)(2,1)S(1)}, bf16[2,8,2048]{2,1,0:T(8,128)(2,1)S(1)}, u32[]{:S(2)}, u32[]{:S(2)}) collective-permute-start(bf16[2,8,2048]{2,1,0:T(8,128)(2,1)S(1)} %get-tuple-element.1520), channel_id=1, source_target_pairs={{0,32},{32,64},{64,96},{96,128},{128,160},{160,192},{192,224},{224... | collective-permute-start | bytes 196616 | tf_op jit(solution)/shard_map/while/body/eval_jaxpr/ppermute | solution.py:13
  469.1 8.0 collective-permute-start.1
  486.4 8.0 collective-permute-start.1
  503.7 8.0 collective-permute-start.1
  521.4 10.8 %collective-permute-start.1 = (bf16[2,8,2048]{2,1,0:T(8,128)(2,1)S(1)}, bf16[2,8,2048]{2,1,0:T(8,128)(2,1)S(1)}, u32[]{:S(2)}, u32[]{:S(2)}) collective-permute-start(bf16[2,8,2048]{2,1,0:T(8,128)(2,1)S(1)} %get-tuple-element.1520), channel_id=1, source_target_pairs={{0,32},{32,64},{64,96},{96,128},{128,160},{160,192},{192,224},{224... | collective-permute-start | bytes 196616 | tf_op jit(solution)/shard_map/while/body/eval_jaxpr/ppermute | solution.py:13
  575.9 8.5 collective-permute-start.1
  593.4 9.0 %collective-permute-start.1 = (bf16[2,8,2048]{2,1,0:T(8,128)(2,1)S(1)}, bf16[2,8,2048]{2,1,0:T(8,128)(2,1)S(1)}, u32[]{:S(2)}, u32[]{:S(2)}) collective-permute-start(bf16[2,8,2048]{2,1,0:T(8,128)(2,1)S(1)} %get-tuple-element.1520), channel_id=1, source_target_pairs={{0,32},{32,64},{64,96},{96,128},{128,160},{160,192},{192,224},{224... | collective-permute-start | bytes 196616 | tf_op jit(solution)/shard_map/while/body/eval_jaxpr/ppermute | solution.py:13
  611.9 8.1 collective-permute-start.1
  629.3 8.0 collective-permute-start.1
  664.6 9.0 %collective-permute-start.1 = (bf16[2,8,2048]{2,1,0:T(8,128)(2,1)S(1)}, bf16[2,8,2048]{2,1,0:T(8,128)(2,1)S(1)}, u32[]{:S(2)}, u32[]{:S(2)}) collective-permute-start(bf16[2,8,2048]{2,1,0:T(8,128)(2,1)S(1)} %get-tuple-element.1520), channel_id=1, source_target_pairs={{0,32},{32,64},{64,96},{96,128},{128,160},{160,192},{192,224},{224... | collective-permute-start | bytes 196616 | tf_op jit(solution)/shard_map/while/body/eval_jaxpr/ppermute | solution.py:13
  675.4 203.8 %all_to_all.5 = bf16[32,8,2048]{2,1,0:T(8,128)(2,1)S(1)} all-to-all(bf16[32,8,2048]{2,1,0:T(8,128)(2,1)S(1)} %bitcast.143), channel_id=1, replica_groups=mesh['pp'=32,'fs'=4,'tp'=8] {'pp'}, dimensions={0} | all-to-all | bytes 2097152 | tf_op jit(solution)/shard_map/all_to_all | solution.py:138
  (1275 shorter events, 460.4 us)
Async XLA Ops:
  6.5 147.4 %all-gather.2.cloned.1.call-start = ((), (), s32[]{:S(2)}) async-start(), calls=%async_computation.1 | async-start | bytes 1081344 | tf_op jit(solution)/shard_map/all_gather | solution.py:121
  342.9 7.4 collective-permute-start
  358.2 7.4 collective-permute-start
  380.9 14.7 %collective-permute-start.1 = (bf16[2,8,2048]{2,1,0:T(8,128)(2,1)S(1)}, bf16[2,8,2048]{2,1,0:T(8,128)(2,1)S(1)}, u32[]{:S(2)}, u32[]{:S(2)}) collective-permute-start(bf16[2,8,2048]{2,1,0:T(8,128)(2,1)S(1)} %get-tuple-element.1520), channel_id=1, source_target_pairs={{0,32},{32,64},{64,96},{96,128},{128,160},{160,192},{192,224},{224... | collective-permute-start | bytes 196616 | tf_op jit(solution)/shard_map/while/body/eval_jaxpr/ppermute | solution.py:13
  403.0 15.0 %collective-permute-start.1 = (bf16[2,8,2048]{2,1,0:T(8,128)(2,1)S(1)}, bf16[2,8,2048]{2,1,0:T(8,128)(2,1)S(1)}, u32[]{:S(2)}, u32[]{:S(2)}) collective-permute-start(bf16[2,8,2048]{2,1,0:T(8,128)(2,1)S(1)} %get-tuple-element.1520), channel_id=1, source_target_pairs={{0,32},{32,64},{64,96},{96,128},{128,160},{160,192},{192,224},{224... | collective-permute-start | bytes 196616 | tf_op jit(solution)/shard_map/while/body/eval_jaxpr/ppermute | solution.py:13
  417.9 7.6 collective-permute-start.1
  425.5 14.5 %collective-permute-start.1 = (bf16[2,8,2048]{2,1,0:T(8,128)(2,1)S(1)}, bf16[2,8,2048]{2,1,0:T(8,128)(2,1)S(1)}, u32[]{:S(2)}, u32[]{:S(2)}) collective-permute-start(bf16[2,8,2048]{2,1,0:T(8,128)(2,1)S(1)} %get-tuple-element.1520), channel_id=1, source_target_pairs={{0,32},{32,64},{64,96},{96,128},{128,160},{160,192},{192,224},{224... | collective-permute-start | bytes 196616 | tf_op jit(solution)/shard_map/while/body/eval_jaxpr/ppermute | solution.py:13
  447.1 14.7 %collective-permute-start.1 = (bf16[2,8,2048]{2,1,0:T(8,128)(2,1)S(1)}, bf16[2,8,2048]{2,1,0:T(8,128)(2,1)S(1)}, u32[]{:S(2)}, u32[]{:S(2)}) collective-permute-start(bf16[2,8,2048]{2,1,0:T(8,128)(2,1)S(1)} %get-tuple-element.1520), channel_id=1, source_target_pairs={{0,32},{32,64},{64,96},{96,128},{128,160},{160,192},{192,224},{224... | collective-permute-start | bytes 196616 | tf_op jit(solution)/shard_map/while/body/eval_jaxpr/ppermute | solution.py:13
  469.1 9.9 %collective-permute-start.1 = (bf16[2,8,2048]{2,1,0:T(8,128)(2,1)S(1)}, bf16[2,8,2048]{2,1,0:T(8,128)(2,1)S(1)}, u32[]{:S(2)}, u32[]{:S(2)}) collective-permute-start(bf16[2,8,2048]{2,1,0:T(8,128)(2,1)S(1)} %get-tuple-element.1520), channel_id=1, source_target_pairs={{0,32},{32,64},{64,96},{96,128},{128,160},{160,192},{192,224},{224... | collective-permute-start | bytes 196616 | tf_op jit(solution)/shard_map/while/body/eval_jaxpr/ppermute | solution.py:13
  486.4 9.9 %collective-permute-start.1 = (bf16[2,8,2048]{2,1,0:T(8,128)(2,1)S(1)}, bf16[2,8,2048]{2,1,0:T(8,128)(2,1)S(1)}, u32[]{:S(2)}, u32[]{:S(2)}) collective-permute-start(bf16[2,8,2048]{2,1,0:T(8,128)(2,1)S(1)} %get-tuple-element.1520), channel_id=1, source_target_pairs={{0,32},{32,64},{64,96},{96,128},{128,160},{160,192},{192,224},{224... | collective-permute-start | bytes 196616 | tf_op jit(solution)/shard_map/while/body/eval_jaxpr/ppermute | solution.py:13
  503.7 10.4 %collective-permute-start.1 = (bf16[2,8,2048]{2,1,0:T(8,128)(2,1)S(1)}, bf16[2,8,2048]{2,1,0:T(8,128)(2,1)S(1)}, u32[]{:S(2)}, u32[]{:S(2)}) collective-permute-start(bf16[2,8,2048]{2,1,0:T(8,128)(2,1)S(1)} %get-tuple-element.1520), channel_id=1, source_target_pairs={{0,32},{32,64},{64,96},{96,128},{128,160},{160,192},{192,224},{224... | collective-permute-start | bytes 196616 | tf_op jit(solution)/shard_map/while/body/eval_jaxpr/ppermute | solution.py:13
  521.4 12.7 %collective-permute-start.1 = (bf16[2,8,2048]{2,1,0:T(8,128)(2,1)S(1)}, bf16[2,8,2048]{2,1,0:T(8,128)(2,1)S(1)}, u32[]{:S(2)}, u32[]{:S(2)}) collective-permute-start(bf16[2,8,2048]{2,1,0:T(8,128)(2,1)S(1)} %get-tuple-element.1520), channel_id=1, source_target_pairs={{0,32},{32,64},{64,96},{96,128},{128,160},{160,192},{192,224},{224... | collective-permute-start | bytes 196616 | tf_op jit(solution)/shard_map/while/body/eval_jaxpr/ppermute | solution.py:13
  541.5 9.6 %collective-permute-start.1 = (bf16[2,8,2048]{2,1,0:T(8,128)(2,1)S(1)}, bf16[2,8,2048]{2,1,0:T(8,128)(2,1)S(1)}, u32[]{:S(2)}, u32[]{:S(2)}) collective-permute-start(bf16[2,8,2048]{2,1,0:T(8,128)(2,1)S(1)} %get-tuple-element.1520), channel_id=1, source_target_pairs={{0,32},{32,64},{64,96},{96,128},{128,160},{160,192},{192,224},{224... | collective-permute-start | bytes 196616 | tf_op jit(solution)/shard_map/while/body/eval_jaxpr/ppermute | solution.py:13
  551.1 7.6 collective-permute-start.1
  558.7 10.1 %collective-permute-start.1 = (bf16[2,8,2048]{2,1,0:T(8,128)(2,1)S(1)}, bf16[2,8,2048]{2,1,0:T(8,128)(2,1)S(1)}, u32[]{:S(2)}, u32[]{:S(2)}) collective-permute-start(bf16[2,8,2048]{2,1,0:T(8,128)(2,1)S(1)} %get-tuple-element.1520), channel_id=1, source_target_pairs={{0,32},{32,64},{64,96},{96,128},{128,160},{160,192},{192,224},{224... | collective-permute-start | bytes 196616 | tf_op jit(solution)/shard_map/while/body/eval_jaxpr/ppermute | solution.py:13
  575.9 10.4 %collective-permute-start.1 = (bf16[2,8,2048]{2,1,0:T(8,128)(2,1)S(1)}, bf16[2,8,2048]{2,1,0:T(8,128)(2,1)S(1)}, u32[]{:S(2)}, u32[]{:S(2)}) collective-permute-start(bf16[2,8,2048]{2,1,0:T(8,128)(2,1)S(1)} %get-tuple-element.1520), channel_id=1, source_target_pairs={{0,32},{32,64},{64,96},{96,128},{128,160},{160,192},{192,224},{224... | collective-permute-start | bytes 196616 | tf_op jit(solution)/shard_map/while/body/eval_jaxpr/ppermute | solution.py:13
  593.4 10.9 %collective-permute-start.1 = (bf16[2,8,2048]{2,1,0:T(8,128)(2,1)S(1)}, bf16[2,8,2048]{2,1,0:T(8,128)(2,1)S(1)}, u32[]{:S(2)}, u32[]{:S(2)}) collective-permute-start(bf16[2,8,2048]{2,1,0:T(8,128)(2,1)S(1)} %get-tuple-element.1520), channel_id=1, source_target_pairs={{0,32},{32,64},{64,96},{96,128},{128,160},{160,192},{192,224},{224... | collective-permute-start | bytes 196616 | tf_op jit(solution)/shard_map/while/body/eval_jaxpr/ppermute | solution.py:13
  604.2 7.7 collective-permute-start.1
  611.9 10.0 %collective-permute-start.1 = (bf16[2,8,2048]{2,1,0:T(8,128)(2,1)S(1)}, bf16[2,8,2048]{2,1,0:T(8,128)(2,1)S(1)}, u32[]{:S(2)}, u32[]{:S(2)}) collective-permute-start(bf16[2,8,2048]{2,1,0:T(8,128)(2,1)S(1)} %get-tuple-element.1520), channel_id=1, source_target_pairs={{0,32},{32,64},{64,96},{96,128},{128,160},{160,192},{192,224},{224... | collective-permute-start | bytes 196616 | tf_op jit(solution)/shard_map/while/body/eval_jaxpr/ppermute | solution.py:13
  629.3 9.9 %collective-permute-start.1 = (bf16[2,8,2048]{2,1,0:T(8,128)(2,1)S(1)}, bf16[2,8,2048]{2,1,0:T(8,128)(2,1)S(1)}, u32[]{:S(2)}, u32[]{:S(2)}) collective-permute-start(bf16[2,8,2048]{2,1,0:T(8,128)(2,1)S(1)} %get-tuple-element.1520), channel_id=1, source_target_pairs={{0,32},{32,64},{64,96},{96,128},{128,160},{160,192},{192,224},{224... | collective-permute-start | bytes 196616 | tf_op jit(solution)/shard_map/while/body/eval_jaxpr/ppermute | solution.py:13
  639.3 7.9 collective-permute-start.1
  647.2 9.6 %collective-permute-start.1 = (bf16[2,8,2048]{2,1,0:T(8,128)(2,1)S(1)}, bf16[2,8,2048]{2,1,0:T(8,128)(2,1)S(1)}, u32[]{:S(2)}, u32[]{:S(2)}) collective-permute-start(bf16[2,8,2048]{2,1,0:T(8,128)(2,1)S(1)} %get-tuple-element.1520), channel_id=1, source_target_pairs={{0,32},{32,64},{64,96},{96,128},{128,160},{160,192},{192,224},{224... | collective-permute-start | bytes 196616 | tf_op jit(solution)/shard_map/while/body/eval_jaxpr/ppermute | solution.py:13
  656.8 7.8 collective-permute-start.1
  664.6 10.8 %collective-permute-start.1 = (bf16[2,8,2048]{2,1,0:T(8,128)(2,1)S(1)}, bf16[2,8,2048]{2,1,0:T(8,128)(2,1)S(1)}, u32[]{:S(2)}, u32[]{:S(2)}) collective-permute-start(bf16[2,8,2048]{2,1,0:T(8,128)(2,1)S(1)} %get-tuple-element.1520), channel_id=1, source_target_pairs={{0,32},{32,64},{64,96},{96,128},{128,160},{160,192},{192,224},{224... | collective-permute-start | bytes 196616 | tf_op jit(solution)/shard_map/while/body/eval_jaxpr/ppermute | solution.py:13
  (200 other events, 632.4 us)
Sparse Core Ops, SparseCore 0:
  10.0 143.9 all-gather.1
where the time goes:
time: 890 us; the launch traced here: 887 us
  starting transfers between devices  303 us (34%)
  waiting for transfers between devices  235 us (26%)
  blocking collectives  204 us (23%)
  matrix products  60.6 us (7%)
  other arithmetic  33.3 us (4%)
  local copies, waits for them, and re-layouts  32 us (4%)
  between operations  13.4 us (2%)
    ppermute x47, starting transfers between devices, passed_along(): return lax.ppermute(x, axis, pairs)  303 us
    all_to_all x1, blocking collectives, shards(): lax.all_to_all(by_slot, 'pp', split_axis=0, concat_axis=0, tiled=True)  204 us
    all_gather x1, waiting for transfers between devices, shards(): everyone = lax.all_gather(tokens_in, 'pp', axis=0, tiled=True)  147 us
    ppermute x47, waiting for transfers between devices, passed_along(): return lax.ppermute(x, axis, pairs)  87.4 us
    dot_general x16, matrix products, run_section(): jnp.dot(flat_rows, w_project, preferred_element_type=jnp.float32)  34.4 us
    dot_general x16, matrix products, run_section(): jnp.dot(mixed_out.reshape(pair_count * length, lru_width), w_back, prefer...  21.5 us
  transfers between devices with their start and end apart: 48, of which 48 were waited for; matrix products, arithmetic and copies ran while one was open for 0% of the time, Pallas kernels for 0%

commit v1 on v0

v1 whole, which is shorter than its diff:
```python
import functools

import jax
import jax.numpy as jnp
from jax import lax
from jax.experimental import pallas as pl
from jax.experimental.pallas import tpu as pltpu
from jax.sharding import PartitionSpec as P

decay_scale = 8.0
norm_eps = 1e-05

pair_stages = 4
group_count = 4
taps = 4


def stages_of(planes):
    paired = 2 * pair_stages
    return pair_stages + (planes - paired) // 4


def plane_of(stage, group, side):
    if stage < pair_stages:
        return 2 * stage + side
    return 2 * pair_stages + 4 * (stage - pair_stages) + 2 * (group % 2) + side


def section(x, weights, vector, at):
    rows, width = x.shape
    length = at.shape[1]
    count = rows // length
    parts, _, chans = weights.shape
    depth = width // parts
    half = chans // 2
    proj = jnp.dot(x[:, :depth], weights[0, :depth, :], preferred_element_type=jnp.float32)
    for t in range(1, parts):
        proj = proj + jnp.dot(
            x[:, t * depth : (t + 1) * depth],
            weights[t, :depth, :],
            preferred_element_type=jnp.float32,
        )
    proj = proj.astype(jnp.bfloat16).astype(jnp.float32).reshape(count, length, chans)
    conv = vector[taps : taps + 1][None] + proj * vector[taps - 1 : taps][None]
    for back in range(1, taps):
        moved = jnp.where(at >= back, pltpu.roll(proj, back, axis=1), 0.0)
        conv = conv + moved * vector[taps - 1 - back : taps - back][None]
    flat = conv.astype(jnp.bfloat16).reshape(rows, chans)
    rate, gate = [], []
    for h in range(2):
        maps = jnp.concatenate(
            [weights[t, 2 * depth :, :] for t in range(h * parts // 2, (h + 1) * parts // 2)], axis=0
        )
        both = jnp.dot(
            flat[:, h * half : (h + 1) * half], maps, preferred_element_type=jnp.float32
        )
        rate.append(both[:, :half])
        gate.append(both[:, half:])
    rate = jnp.concatenate(rate, axis=1) + vector[5:6]
    gate = jnp.concatenate(gate, axis=1) + vector[6:7]
    rate = 1.0 / (1.0 + jnp.exp(-rate))
    gate = 1.0 / (1.0 + jnp.exp(-gate))
    log_decay = rate * vector[7:8]
    lost = 1.0 + log_decay * (1.0 / 7.0)
    for k in (6.0, 5.0, 4.0, 3.0, 2.0):
        lost = 1.0 + log_decay * (1.0 / k) * lost
    lost = lost * log_decay
    hidden = jnp.sqrt(-lost * (2.0 + lost)) * gate * flat.astype(jnp.float32)
    decay = (1.0 + lost).reshape(count, length, chans)
    hidden = hidden.reshape(count, length, chans)
    back = 1
    while back < length:
        hidden = hidden + decay * jnp.where(at >= back, pltpu.roll(hidden, back, axis=1), 0.0)
        if 2 * back < length:
            decay = decay * jnp.where(at >= back, pltpu.roll(decay, back, axis=1), 1.0)
        back = 2 * back
    mixed = hidden.astype(jnp.bfloat16).reshape(rows, chans)
    update = [
        jnp.dot(mixed[:, :half], weights[t, depth : 2 * depth, :half], preferred_element_type=jnp.float32)
        + jnp.dot(mixed[:, half:], weights[t, depth : 2 * depth, half:], preferred_element_type=jnp.float32)
        for t in range(parts)
    ]
    summed = x.astype(jnp.float32) + jnp.concatenate(update, axis=1)
    mean_value = jnp.mean(summed, axis=1, keepdims=True)
    centered = summed - mean_value
    variance = jnp.mean(centered * centered, axis=1, keepdims=True)
    lines = width // chans
    gain = jnp.concatenate([vector[8 + q : 9 + q] for q in range(lines)], axis=1)
    shift = jnp.concatenate([vector[8 + lines + q : 9 + lines + q] for q in range(lines)], axis=1)
    normed = centered * lax.rsqrt(variance + norm_eps) * gain + shift
    return normed.astype(jnp.bfloat16)


def stage_kernel(step, length, both, enters, *refs):
    x_ref, own_ref, own_vectors = refs[:3]
    o_ref = refs[-1]
    plane = lax.axis_index("pp")
    paired = 2 * pair_stages
    mine = lax.div(lax.rem(plane, 4), 2)
    in_pair = plane < paired
    stage = jnp.where(in_pair, lax.div(plane, 2), pair_stages + lax.div(plane - paired, 4))
    group = step - 2 * stage
    active = (group >= 0) & (group < group_count)
    active = active & (in_pair | (lax.rem(group + 2 * group_count, 2) == mine))
    first = jnp.where(in_pair, 2 * mine, 0)
    last = jnp.where(active, jnp.where(in_pair, 2 * mine + 2, 4), first)
    if enters:
        o_ref[...] = jnp.where(plane < 2, refs[-2][...], x_ref[...])
    else:
        o_ref[...] = x_ref[...]
    rows = x_ref.shape[0]
    chans = own_vectors.shape[2]
    at = lax.broadcasted_iota(jnp.int32, (rows // length, length, chans), 1)

    def run(weights, vectors, j):
        o_ref[...] = section(o_ref[...], weights.at[:, j], vectors[j], at)

    def one(j, unused):
        if not both:
            run(own_ref, own_vectors, lax.rem(j, 2))
            return unused

        @pl.when(lax.div(j, 2) == mine)
        def _():
            run(own_ref, own_vectors, lax.rem(j, 2))

        @pl.when(lax.div(j, 2) != mine)
        def _():
            run(refs[3], refs[4], lax.rem(j, 2))

        return unused

    lax.fori_loop(first, last, one, 0)


def run_stage(step, length, x, entry, own, other):
    operands = (x,) + own + (other if other is not None else ()) + (() if entry is None else (entry,))
    rows, width = x.shape
    chans = own[1].shape[2]
    sections = 2 if other is None else 4
    spec = pl.BlockSpec(memory_space=pltpu.VMEM)
    return pl.pallas_call(
        functools.partial(stage_kernel, step, length, other is not None, entry is not None),
        out_shape=jax.ShapeDtypeStruct(x.shape, x.dtype),
        in_specs=[spec] * len(operands),
        out_specs=spec,
        compiler_params=pltpu.CompilerParams(vmem_limit_bytes=24 << 20),
        cost_estimate=pl.CostEstimate(
            flops=4 * sections * rows * width * chans,
            bytes_accessed=sections * 4 * width * chans,
            transcendentals=sections * 5 * rows * chans,
        ),
        name="stage",
    )(*operands)


def join_kernel(mine_ref, near_ref, o_ref, done):
    odd = lax.rem(lax.axis_index("pp"), 2)
    copies = [
        pltpu.make_async_copy(mine_ref, o_ref.at[:, odd], done.at[0]),
        pltpu.make_async_copy(near_ref, o_ref.at[:, 1 - odd], done.at[1]),
    ]
    for copy in copies:
        copy.start()
    for copy in copies:
        copy.wait()


def joined(mine, near):
    parts, lines, chans = mine.shape
    return pl.pallas_call(
        join_kernel,
        out_shape=jax.ShapeDtypeStruct((parts, 2, lines, chans), mine.dtype),
        in_specs=[pl.BlockSpec(memory_space=pl.ANY)] * 2,
        out_specs=pl.BlockSpec(memory_space=pltpu.VMEM),
        scratch_shapes=[pltpu.SemaphoreType.DMA((2,))],
        compiler_params=pltpu.CompilerParams(vmem_limit_bytes=12 << 20),
        name="join",
    )(mine, near)


def packed_weights(w_project, w_back, gate_rate, gate_input, parts):
    width, chans = w_project.shape
    depth, half, block = width // parts, chans // 2, gate_rate.shape[1]
    project = w_project.reshape(parts, depth, chans)
    back = w_back.reshape(2, half, parts, depth).transpose(2, 1, 0, 3).reshape(parts, half, 2 * depth)
    place = jnp.arange(parts)[:, None] % (parts // 2) == jnp.arange(parts // 2)[None, :]
    maps = jnp.stack([gate_rate, gate_input], axis=2)[:, :, :, None, :]
    maps = jnp.where(place[:, None, None, :, None], maps, jnp.zeros((), maps.dtype))
    return jnp.concatenate([project, back, maps.reshape(parts, block, chans)], axis=1)


def packed_shard(w_project, w_back, gate_rate, gate_input, parts):
    width, chans = w_project.shape
    depth, half, block = width // parts, chans // 2, gate_rate.shape[1]
    part = lax.axis_index("tp")
    project = lax.dynamic_slice_in_dim(w_project, part * depth, depth, 0)
    back = lax.dynamic_slice_in_dim(w_back, part * depth, depth, 1)
    back = jnp.concatenate([back[:half], back[half:]], axis=1)
    maps = [lax.dynamic_index_in_dim(g, part, 0, keepdims=False) for g in (gate_rate, gate_input)]
    place = (jnp.arange(half) // block) == part % (parts // 2)
    maps = [jnp.where(place, jnp.tile(g, (1, half // block)), jnp.zeros((), g.dtype)) for g in maps]
    return jnp.concatenate([project, back, jnp.concatenate(maps, axis=1)], axis=0)


def shards(
    tokens_in,
    weight_in,
    conv_taps,
    conv_bias,
    gate_rate,
    bias_rate,
    gate_input,
    bias_input,
    decay_param,
    weight_out,
    norm_gain,
    norm_shift,
):
    planes = lax.axis_size("pp")
    parts = lax.axis_size("tp")
    splits = lax.axis_size("fs")
    plane = lax.axis_index("pp")
    length, width = tokens_in.shape[2:]
    chans = weight_in.shape[2]
    odd = plane % 2
    paired = 2 * pair_stages

    def moved(x, pairs):
        return lax.ppermute(x, "pp", [(int(a), int(b)) for a, b in pairs])

    def in_order(mine, theirs):
        return jnp.stack(
            [jnp.where(odd == 0, mine, theirs), jnp.where(odd == 0, theirs, mine)], axis=0
        )

    packed = packed_weights(weight_in[0], weight_out[0], gate_rate[0], gate_input[0], parts)
    shard = packed_shard(weight_in[0], weight_out[0], gate_rate[0], gate_input[0], parts)
    swap = [(i, i ^ 1) for i in range(planes)]
    shard_near = moved(shard, swap)
    vector = jnp.concatenate(
        [
            conv_taps[0],
            conv_bias,
            bias_rate,
            bias_input,
            -decay_scale * jax.nn.softplus(-decay_param),
            norm_gain.reshape(-1, chans),
            norm_shift.reshape(-1, chans),
        ],
        axis=0,
    )
    vector_near = moved(vector, swap)
    near = lax.all_gather(shard_near, "tp", axis=0)
    own_vectors = in_order(vector, vector_near)

    across = [(i, i ^ 2) for i in range(paired, planes)]
    couple = in_order(shard, shard_near)
    lines = shard.shape[0] // splits
    piece = lax.dynamic_slice_in_dim(couple, lax.axis_index("fs") * lines, lines, 1)
    piece = moved(piece, across)
    other_vectors = moved(own_vectors, across)

    token = tokens_in.reshape(length, width)
    span = planes // group_count
    per = span // 2
    bases = [(g, s) for g in range(group_count) for s in range(2)]
    collected = jnp.concatenate(
        [token]
        + [moved(token, [(span * g + s + 2 * q, span * g + s) for g, s in bases]) for q in range(1, per)],
        axis=0,
    )
    entries = [collected] + [
        moved(collected, [(span * g + s, s) for s in range(2)]) for g in range(1, group_count)
    ]

    packed, collected, entries[1], piece, other_vectors, near = lax.optimization_barrier(
        (packed, collected, entries[1], piece, other_vectors, near)
    )
    entries[0] = collected
    own = joined(packed, near)
    other = lax.all_gather(piece, "fs", axis=1, tiled=True)

    stages = stages_of(planes)
    outputs, arrived = [], []
    for step in range(2 * stages + group_count - 2):
        x = arrived[step - 2] if step >= 2 else None
        entry = entries[step] if step < group_count else None
        if x is None:
            x, entry = entry, None
        if step == 1:
            x = lax.optimization_barrier((x, outputs[0]))[0]
        late = step >= 2 * pair_stages
        y = run_stage(
            step, length, x, entry, (own, own_vectors), (other, other_vectors) if late else None
        )
        pairs = [
            (plane_of(i, step - 2 * i, s), plane_of(i + 1, step - 2 * i, s))
            for i in range(stages - 1)
            if 0 <= step - 2 * i < group_count
            for s in range(2)
        ]
        if step == 2:
            other = lax.optimization_barrier((other, outputs[1], y))[0]
            other = lax.all_gather(other, "tp", axis=0)
        arrived.append(moved(y, pairs) if pairs else None)
        outputs.append(y)

    last = stages - 1
    stay = [plane_of(last, group_count - 1, s) for s in range(2)]
    done = outputs[-1]
    early = None
    parts_in = [
        moved(outputs[2 * last + g], [(plane_of(last, g, s), span * g + s) for s in range(2)])
        for g in range(group_count - 1)
    ]
    parts_in, done = lax.optimization_barrier((parts_in, done))
    for part in parts_in:
        early = part if early is None else early + part
    at_end = plane >= stay[0]
    done = jnp.where(at_end, done, early).reshape(per, length, width)
    final = None
    for c in range(1, per):
        send = jnp.where(at_end, done[c - 1], done[c])
        pairs = [
            (span * g + s, span * g + s + 2 * c) for g in range(group_count - 1) for s in range(2)
        ] + [(stay[s], span * (group_count - 1) + s + 2 * (c - 1)) for s in range(2)]
        part = moved(send, pairs)
        final = part if final is None else final + part
    keeps = at_end | ((plane % span < 2) & (plane < span * (group_count - 1)))
    final = jnp.where(keeps, jnp.where(at_end, done[per - 1], done[0]), final)
    return final.reshape(1, 1, length, width)


def solution(mesh):
    placed = (
        P("pp", ("fs", "tp"), None, None),
        P("pp", None, None),
        P("pp", None, None),
        P("pp", None),
        P("pp", None, None, None),
        P("pp", None),
        P("pp", None, None, None),
        P("pp", None),
        P("pp", None),
        P("pp", None, None),
        P("pp", None),
        P("pp", None),
    )
    return jax.shard_map(
        shards,
        mesh=mesh,
        in_specs=placed,
        out_specs=P("pp", ("fs", "tp"), None, None),
        check_vma=False,
    )
```

time: 890 us -> 331 us (0.37)
  the two profiles are of different devices: /device:TPU:6 before, /device:TPU:928 now
where the time goes in v1:
time: 331 us; the launch traced here: 330 us
  waiting for transfers between devices  207 us (63%)
  starting transfers between devices  44.2 us (13%)
  local copies, waits for them, and re-layouts  41.6 us (13%)
  between operations  14.3 us (4%)
  Pallas kernels  12.8 us (4%)
  other arithmetic  10.1 us (3%)
    ppermute x36, waiting for transfers between devices, moved(): return lax.ppermute(x, 'pp', [(int(a), int(b)) for a, b in pairs])  101 us
    all_gather x1, waiting for transfers between devices, shards(): other = lax.all_gather(other, 'tp', axis=0)  65.9 us
    ppermute x36, starting transfers between devices, moved(): return lax.ppermute(x, 'pp', [(int(a), int(b)) for a, b in pairs])  44.1 us
    all_gather x1, waiting for transfers between devices, shards(): other = lax.all_gather(piece, 'fs', axis=1, tiled=True)  35.4 us
    unnamed x64, local copies, waits for them, and re-layouts  31.4 us
    pallas_call x22, Pallas kernels, run_stage(): pl.pallas_call(functools.partial(stage_kernel, step, length, other is not...  12.1 us
  transfers between devices with their start and end apart: 39, of which 8 were waited for; matrix products, arithmetic and copies ran while one was open for 5% of the time, Pallas kernels for 4%

profile of v1, /device:TPU:928, one launch (start us, length us, event | category | flops | bytes accessed | tf_op | source)
XLA Modules:
  0.0 329.9 jit_solution(5862454125758199362)
XLA Ops:
  10.4 2.9 collective-permute-start.4
  13.4 14.0 %collective-permute-done.4 = bf16[576,512]{1,0:T(8,128)(2,1)S(1)} collective-permute-done((bf16[576,512]{1,0:T(8,128)(2,1)S(1)}, bf16[576,512]{1,0:T(8,128)(2,1)S(1)}, u32[]{:S(2)}, u32[]{:S(2)}) %collective-permute-start.4) | collective-permute-done | bytes 589856 | tf_op jit(solution)/shard_map/ppermute | solution.py:230
  29.5 6.1 %collective-permute-start.1 = (bf16[8,2048]{1,0:T(8,128)(2,1)}, bf16[8,2048]{1,0:T(8,128)(2,1)}, u32[]{:S(2)}, u32[]{:S(2)}) collective-permute-start(bf16[8,2048]{1,0:T(8,128)(2,1)} %bitcast.4), channel_id=1, source_target_pairs={{128,0},{160,32},{384,256},{416,288},{640,512},{672,544},{896,768}... | collective-permute-start | bytes 98312 | tf_op jit(solution)/shard_map/ppermute | solution.py:230
  38.8 2.9 collective-permute-start.6
  48.9 2.6 reshape.81
  52.3 4.6 %collective-permute-start.7 = (f32[2,16,512]{2,1,0:T(8,128)S(1)}, f32[2,16,512]{2,1,0:T(8,128)S(1)}, u32[]{:S(2)}, u32[]{:S(2)}) collective-permute-start(f32[2,16,512]{2,1,0:T(8,128)S(1)} %pad_maximum_fusion.3.refs_2_), channel_id=1, source_target_pairs={{256,320},{288,352},{320,256},{352,288},{384,448},{416,480},{448,3... | collective-permute-start | bytes 196616 | tf_op jit(solution)/shard_map/ppermute | solution.py:230
  59.7 2.4 collective-permute-start.5
  62.1 3.4 %pad_maximum_fusion.mine_ref = bf16[8,576,512]{2,1,0:T(8,128)(2,1)} fusion(bf16[8,64,512]{2,1,0:T(8,128)(2,1)} %broadcast_select_fusion, bf16[8,256,512]{2,1,0:T(8,128)(2,1)S(1)} %copy-done.9, bf16[8,256,512]{2,1,0:T(8,128)(2,1)S(1)} %bitcast.52), kind=kLoop, calls=%fused_computation | loop fusion | flops 14155776 | bytes 9437184 | tf_op jit(solution)/shard_map/concatenate | solution.py:190
  65.5 7.5 %collective-permute-done.5 = bf16[2,144,512]{2,1,0:T(8,128)(2,1)S(1)} collective-permute-done((bf16[2,144,512]{2,1,0:T(8,128)(2,1)S(1)}, bf16[2,144,512]{2,1,0:T(8,128)(2,1)S(1)}, u32[]{:S(2)}, u32[]{:S(2)}) %collective-permute-start.5) | collective-permute-done | bytes 294944 | tf_op jit(solution)/shard_map/ppermute | solution.py:230
  73.0 4.5 %all-gather.8.cloned.1.call-done = bf16[4608,512]{1,0:T(8,128)(2,1)} async-done(((bf16[576,512]{1,0:T(8,128)(2,1)}), bf16[4608,512]{1,0:T(8,128)(2,1)}) %all-gather.8.cloned.1.call-update) | async-done | bytes 4718608 | tf_op jit(solution)/shard_map/all_gather | solution.py:254
  84.3 2.9 copy-done
  87.2 35.4 %all-gather.6.cloned.1.call-done = bf16[2,576,512]{2,1,0:T(8,128)(2,1)} async-done(((bf16[2,144,512]{2,1,0:T(8,128)(2,1)}), bf16[2,576,512]{2,1,0:T(8,128)(2,1)}) %all-gather.6.cloned.1.call-update) | async-done | bytes 1179664 | tf_op jit(solution)/shard_map/all_gather | solution.py:282
  124.7 3.7 %copy-done.1 = bf16[8,2,576,512]{3,2,1,0:T(8,128)(2,1)S(1)} copy-done((bf16[8,2,576,512]{3,2,1,0:T(8,128)(2,1)S(1)}, bf16[8,2,576,512]{3,2,1,0:T(8,128)(2,1)}, u32[]{:S(2)}) %copy-start.1) | copy-done | bytes 9437208
  132.2 65.9 %all-gather.10.cloned.1.call-done = bf16[16,576,512]{2,1,0:T(8,128)(2,1)} async-done(((bf16[2,576,512]{2,1,0:T(8,128)(2,1)}), bf16[16,576,512]{2,1,0:T(8,128)(2,1)}) %all-gather.10.cloned.1.call-update) | async-done | bytes 9437200 | tf_op jit(solution)/shard_map/all_gather | solution.py:305
  198.1 3.7 %copy-done.2 = bf16[8,2,576,512]{3,2,1,0:T(8,128)(2,1)S(1)} copy-done((bf16[8,2,576,512]{3,2,1,0:T(8,128)(2,1)S(1)}, bf16[8,2,576,512]{3,2,1,0:T(8,128)(2,1)}, u32[]{:S(2)}) %copy-start.2) | copy-done | bytes 9437208
  201.8 3.7 %copy-done.4 = bf16[16,576,512]{2,1,0:T(8,128)(2,1)S(1)} copy-done((bf16[16,576,512]{2,1,0:T(8,128)(2,1)S(1)}, bf16[16,576,512]{2,1,0:T(8,128)(2,1)}, u32[]{:S(2)}) %copy-start.4) | copy-done | bytes 9437208
  206.3 2.8 copy-done.5
  216.5 63.0 %collective-permute-done.17.refs_0_ = bf16[32,2048]{1,0:T(8,128)(2,1)S(1)} collective-permute-done((bf16[32,2048]{1,0:T(8,128)(2,1)S(1)}, bf16[32,2048]{1,0:T(8,128)(2,1)S(1)}, u32[]{:S(2)}, u32[]{:S(2)}) %collective-permute-start.17) | collective-permute-done | bytes 131104 | tf_op jit(solution)/shard_map/ppermute | solution.py:230
  279.5 5.6 %stage.32 = bf16[32,2048]{1,0:T(8,128)(2,1)S(1)} custom-call(bf16[32,2048]{1,0:T(8,128)(2,1)S(1)} %collective-permute-done.17.refs_0_, bf16[8,2,576,512]{3,2,1,0:T(8,128)(2,1)S(1)} %copy-done.2, f32[2,16,512]{2,1,0:T(8,128)S(1)} %pad_maximum_fusion.3.refs_2_, bf16[8,2,576,512]{3,2,1,0:T(8,128)(2,1)S(1)} %bitcast.44, ...), custom_call_target="tpu_custom_call" | custom-call | flops 536870912 | bytes 16777216 | tf_op jit(solution)/shard_map/stage/pallas_call | solution.py:142
  289.1 6.9 %collective-permute-done.30.refs_0_ = bf16[32,2048]{1,0:T(8,128)(2,1)S(1)} collective-permute-done((bf16[32,2048]{1,0:T(8,128)(2,1)S(1)}, bf16[32,2048]{1,0:T(8,128)(2,1)S(1)}, u32[]{:S(2)}, u32[]{:S(2)}) %collective-permute-start.30) | collective-permute-done | bytes 131104 | tf_op jit(solution)/shard_map/ppermute | solution.py:230
  296.0 5.6 %stage.42 = bf16[32,2048]{1,0:T(8,128)(2,1)S(1)} custom-call(bf16[32,2048]{1,0:T(8,128)(2,1)S(1)} %collective-permute-done.30.refs_0_, bf16[8,2,576,512]{3,2,1,0:T(8,128)(2,1)S(1)} %copy-done.2, f32[2,16,512]{2,1,0:T(8,128)S(1)} %pad_maximum_fusion.3.refs_2_, bf16[8,2,576,512]{3,2,1,0:T(8,128)(2,1)S(1)} %bitcast.46, ...), custom_call_target="tpu_custom_call" | custom-call | flops 536870912 | bytes 16777216 | tf_op jit(solution)/shard_map/stage/pallas_call | solution.py:142
  302.9 3.7 %copy-done.3 = bf16[8,2,576,512]{3,2,1,0:T(8,128)(2,1)S(1)} copy-done((bf16[8,2,576,512]{3,2,1,0:T(8,128)(2,1)S(1)}, bf16[8,2,576,512]{3,2,1,0:T(8,128)(2,1)}, u32[]{:S(2)}) %copy-start.3) | copy-done | bytes 9437208
  306.6 3.7 %copy-done.6 = bf16[16,576,512]{2,1,0:T(8,128)(2,1)S(1)} copy-done((bf16[16,576,512]{2,1,0:T(8,128)(2,1)S(1)}, bf16[16,576,512]{2,1,0:T(8,128)(2,1)}, u32[]{:S(2)}) %copy-start.6) | copy-done | bytes 9437208
  313.1 9.6 %collective-permute-done.35 = bf16[8,2048]{1,0:T(8,128)(2,1)S(1)} collective-permute-done((bf16[8,2048]{1,0:T(8,128)(2,1)S(1)}, bf16[8,2048]{1,0:T(8,128)(2,1)S(1)}, u32[]{:S(2)}, u32[]{:S(2)}) %collective-permute-start.35) | collective-permute-done | bytes 32800 | tf_op jit(solution)/shard_map/ppermute | solution.py:230
  (180 shorter events, 48.7 us)
Async XLA Ops:
  6.6 70.9 %all-gather.8.cloned.1.call-start = ((), (), s32[]{:S(2)}) async-start(), calls=%async_computation.1 | async-start | bytes 5308416 | tf_op jit(solution)/shard_map/all_gather | solution.py:254
  10.4 16.9 %collective-permute-start.4 = (bf16[576,512]{1,0:T(8,128)(2,1)S(1)}, bf16[576,512]{1,0:T(8,128)(2,1)S(1)}, u32[]{:S(2)}, u32[]{:S(2)}) collective-permute-start(bf16[576,512]{1,0:T(8,128)(2,1)S(1)} %maximum_maximum_fusion), channel_id=1, source_target_pairs={{0,32},{32,0},{64,96},{96,64},{128,160},{160,128},{192,224},{224,1... | collective-permute-start | bytes 1769480 | tf_op jit(solution)/shard_map/ppermute | solution.py:230
  28.2 94.4 %all-gather.6.cloned.1.call-start = ((), (), s32[]{:S(2)}) async-start(), calls=%async_computation | async-start | bytes 1474560 | tf_op jit(solution)/shard_map/all_gather | solution.py:282
  28.3 28.7 %collective-permute-start = (bf16[8,2048]{1,0:T(8,128)(2,1)}, bf16[8,2048]{1,0:T(8,128)(2,1)}, u32[]{:S(2)}, u32[]{:S(2)}) collective-permute-start(bf16[8,2048]{1,0:T(8,128)(2,1)} %bitcast.4), channel_id=1, source_target_pairs={{64,0},{96,32},{320,256},{352,288},{576,512},{608,544},{832,768},{... | collective-permute-start | bytes 98312 | tf_op jit(solution)/shard_map/ppermute | solution.py:230
  29.5 27.4 %collective-permute-start.1 = (bf16[8,2048]{1,0:T(8,128)(2,1)}, bf16[8,2048]{1,0:T(8,128)(2,1)}, u32[]{:S(2)}, u32[]{:S(2)}) collective-permute-start(bf16[8,2048]{1,0:T(8,128)(2,1)} %bitcast.4), channel_id=1, source_target_pairs={{128,0},{160,32},{384,256},{416,288},{640,512},{672,544},{896,768}... | collective-permute-start | bytes 98312 | tf_op jit(solution)/shard_map/ppermute | solution.py:230
  35.6 21.3 %collective-permute-start.2 = (bf16[8,2048]{1,0:T(8,128)(2,1)}, bf16[8,2048]{1,0:T(8,128)(2,1)}, u32[]{:S(2)}, u32[]{:S(2)}) collective-permute-start(bf16[8,2048]{1,0:T(8,128)(2,1)} %bitcast.4), channel_id=1, source_target_pairs={{192,0},{224,32},{448,256},{480,288},{704,512},{736,544},{960,768}... | collective-permute-start | bytes 98312 | tf_op jit(solution)/shard_map/ppermute | solution.py:230
  38.8 12.8 %collective-permute-start.6 = (f32[16,512]{1,0:T(8,128)S(1)}, f32[16,512]{1,0:T(8,128)}, u32[]{:S(2)}, u32[]{:S(2)}) collective-permute-start(f32[16,512]{1,0:T(8,128)S(1)} %concatenate.23), channel_id=1, source_target_pairs={{0,32},{32,0},{64,96},{96,64},{128,160},{160,128},{192,224},{224,1... | collective-permute-start | bytes 98312 | tf_op jit(solution)/shard_map/ppermute | solution.py:230
  52.3 13.2 %collective-permute-start.7 = (f32[2,16,512]{2,1,0:T(8,128)S(1)}, f32[2,16,512]{2,1,0:T(8,128)S(1)}, u32[]{:S(2)}, u32[]{:S(2)}) collective-permute-start(f32[2,16,512]{2,1,0:T(8,128)S(1)} %pad_maximum_fusion.3.refs_2_), channel_id=1, source_target_pairs={{256,320},{288,352},{320,256},{352,288},{384,448},{416,480},{448,3... | collective-permute-start | bytes 196616 | tf_op jit(solution)/shard_map/ppermute | solution.py:230
  57.8 7.7 %collective-permute-start.3 = (bf16[32,2048]{1,0:T(8,128)(2,1)S(1)}, bf16[32,2048]{1,0:T(8,128)(2,1)S(1)}, u32[]{:S(2)}, u32[]{:S(2)}) collective-permute-start(bf16[32,2048]{1,0:T(8,128)(2,1)S(1)} %pad_maximum_fusion.2.refs_0_), channel_id=1, source_target_pairs={{256,0},{288,32},{257,1},{289,33},{258,2},{290,34},{259,3},{291,35... | collective-permute-start | bytes 393224 | tf_op jit(solution)/shard_map/ppermute | solution.py:230
  59.7 13.3 %collective-permute-start.5 = (bf16[2,144,512]{2,1,0:T(8,128)(2,1)S(1)}, bf16[2,144,512]{2,1,0:T(8,128)(2,1)S(1)}, u32[]{:S(2)}, u32[]{:S(2)}) collective-permute-start(bf16[2,144,512]{2,1,0:T(8,128)(2,1)S(1)} %fusion), channel_id=1, source_target_pairs={{256,320},{288,352},{320,256},{352,288},{384,448},{416,480},{448,3... | collective-permute-start | bytes 884744 | tf_op jit(solution)/shard_map/ppermute | solution.py:230
  77.5 120.6 %all-gather.10.cloned.1.call-start = ((), (), s32[]{:S(2)}) async-start(), calls=%async_computation.2 | async-start | bytes 10616832 | tf_op jit(solution)/shard_map/all_gather | solution.py:305
  77.5 6.8 %collective-permute-start.9 = (bf16[32,2048]{1,0:T(8,128)(2,1)S(1)}, bf16[32,2048]{1,0:T(8,128)(2,1)S(1)}, u32[]{:S(2)}, u32[]{:S(2)}) collective-permute-start(bf16[32,2048]{1,0:T(8,128)(2,1)S(1)} %pad_maximum_fusion.2.refs_0_), channel_id=1, source_target_pairs={{512,0},{544,32},{513,1},{545,33},{514,2},{546,34},{515,3},{547,35... | collective-permute-start | bytes 393224 | tf_op jit(solution)/shard_map/ppermute | solution.py:230
  124.0 5.1 %collective-permute-start.10 = (bf16[32,2048]{1,0:T(8,128)(2,1)S(1)}, bf16[32,2048]{1,0:T(8,128)(2,1)S(1)}, u32[]{:S(2)}, u32[]{:S(2)}) collective-permute-start(bf16[32,2048]{1,0:T(8,128)(2,1)S(1)} %stage.23), channel_id=1, source_target_pairs={{0,64},{32,96},{64,128},{96,160},{1,65},{33,97},{65,129},{97,161},... | collective-permute-start | bytes 393224 | tf_op jit(solution)/shard_map/ppermute | solution.py:230
  131.5 74.8 %collective-permute-start.23 = (bf16[32,2048]{1,0:T(8,128)(2,1)S(1)}, bf16[32,2048]{1,0:T(8,128)(2,1)S(1)}, u32[]{:S(2)}, u32[]{:S(2)}) collective-permute-start(bf16[32,2048]{1,0:T(8,128)(2,1)S(1)} %stage.35), channel_id=1, source_target_pairs={{128,192},{160,224},{192,320},{224,352},{129,193},{161,225},{193,3... | collective-permute-start | bytes 393224 | tf_op jit(solution)/shard_map/ppermute | solution.py:230
  205.5 4.4 %collective-permute-start.13 = (bf16[32,2048]{1,0:T(8,128)(2,1)S(1)}, bf16[32,2048]{1,0:T(8,128)(2,1)S(1)}, u32[]{:S(2)}, u32[]{:S(2)}) collective-permute-start(bf16[32,2048]{1,0:T(8,128)(2,1)S(1)} %stage.27), channel_id=1, source_target_pairs={{192,256},{224,288},{256,384},{288,416},{193,257},{225,289},{257,3... | collective-permute-start | bytes 393224 | tf_op jit(solution)/shard_map/ppermute | solution.py:230
  214.5 65.1 %collective-permute-start.17 = (bf16[32,2048]{1,0:T(8,128)(2,1)S(1)}, bf16[32,2048]{1,0:T(8,128)(2,1)S(1)}, u32[]{:S(2)}, u32[]{:S(2)}) collective-permute-start(bf16[32,2048]{1,0:T(8,128)(2,1)S(1)} %stage.31), channel_id=1, source_target_pairs={{640,768},{672,800},{768,896},{800,928},{641,769},{673,801},{769,8... | collective-permute-start | bytes 393224 | tf_op jit(solution)/shard_map/ppermute | solution.py:230
  215.8 70.6 %collective-permute-start.28 = (bf16[32,2048]{1,0:T(8,128)(2,1)S(1)}, bf16[32,2048]{1,0:T(8,128)(2,1)S(1)}, u32[]{:S(2)}, u32[]{:S(2)}) collective-permute-start(bf16[32,2048]{1,0:T(8,128)(2,1)S(1)} %stage.40), channel_id=1, source_target_pairs={{704,832},{736,864},{832,960},{864,992},{705,833},{737,865},{833,9... | collective-permute-start | bytes 393224 | tf_op jit(solution)/shard_map/ppermute | solution.py:230
  285.1 10.9 %collective-permute-start.30 = (bf16[32,2048]{1,0:T(8,128)(2,1)S(1)}, bf16[32,2048]{1,0:T(8,128)(2,1)S(1)}, u32[]{:S(2)}, u32[]{:S(2)}) collective-permute-start(bf16[32,2048]{1,0:T(8,128)(2,1)S(1)} %stage.32), channel_id=1, source_target_pairs={{768,896},{800,928},{769,897},{801,929},{770,898},{802,930},{771,8... | collective-permute-start | bytes 393224 | tf_op jit(solution)/shard_map/ppermute | solution.py:230
  286.5 16.5 %collective-permute-start.32 = (bf16[32,2048]{1,0:T(8,128)(2,1)S(1)}, bf16[32,2048]{1,0:T(8,128)(2,1)S(1)}, u32[]{:S(2)}, u32[]{:S(2)}) collective-permute-start(bf16[32,2048]{1,0:T(8,128)(2,1)S(1)} %stage.41), channel_id=1, source_target_pairs={{832,960},{864,992},{833,961},{865,993},{834,962},{866,994},{835,9... | collective-permute-start | bytes 393224 | tf_op jit(solution)/shard_map/ppermute | solution.py:230
  287.1 23.2 %collective-permute-start.29 = (bf16[32,2048]{1,0:T(8,128)(2,1)S(1)}, bf16[32,2048]{1,0:T(8,128)(2,1)S(1)}, u32[]{:S(2)}, u32[]{:S(2)}) collective-permute-start(bf16[32,2048]{1,0:T(8,128)(2,1)S(1)} %stage.41), channel_id=1, source_target_pairs={{960,256},{992,288},{961,257},{993,289},{962,258},{994,290},{963,2... | collective-permute-start | bytes 393224 | tf_op jit(solution)/shard_map/ppermute | solution.py:230
  287.8 22.5 %collective-permute-start.18 = (bf16[32,2048]{1,0:T(8,128)(2,1)S(1)}, bf16[32,2048]{1,0:T(8,128)(2,1)S(1)}, u32[]{:S(2)}, u32[]{:S(2)}) collective-permute-start(bf16[32,2048]{1,0:T(8,128)(2,1)S(1)} %stage.32), channel_id=1, source_target_pairs={{896,0},{928,32},{897,1},{929,33},{898,2},{930,34},{899,3},{931,35... | collective-permute-start | bytes 393224 | tf_op jit(solution)/shard_map/ppermute | solution.py:230
  301.6 8.7 %collective-permute-start.31 = (bf16[32,2048]{1,0:T(8,128)(2,1)S(1)}, bf16[32,2048]{1,0:T(8,128)(2,1)S(1)}, u32[]{:S(2)}, u32[]{:S(2)}) collective-permute-start(bf16[32,2048]{1,0:T(8,128)(2,1)S(1)} %stage.42), channel_id=1, source_target_pairs={{896,512},{928,544},{897,513},{929,545},{898,514},{930,546},{899,5... | collective-permute-start | bytes 393224 | tf_op jit(solution)/shard_map/ppermute | solution.py:230
  310.4 2.7 collective-permute-start.33
  311.8 11.0 %collective-permute-start.35 = (bf16[8,2048]{1,0:T(8,128)(2,1)S(1)}, bf16[8,2048]{1,0:T(8,128)(2,1)S(1)}, u32[]{:S(2)}, u32[]{:S(2)}) collective-permute-start(bf16[8,2048]{1,0:T(8,128)(2,1)S(1)} %get-tuple-element.35), channel_id=1, source_target_pairs={{0,192},{32,224},{256,448},{288,480},{512,704},{544,736},{960,896}... | collective-permute-start | bytes 98312 | tf_op jit(solution)/shard_map/ppermute | solution.py:230
  (46 other events, 425.1 us)
Sparse Core Ops, SparseCore 0:
  28.3 49.0 all-gather.7
  80.1 42.4 all-gather.5
  125.4 72.6 all-gather.9

commit v2 on v1

--- a/solution.py
+++ b/solution.py
@@ -91,8 +91,7 @@
     return normed.astype(jnp.bfloat16)
 
 
-def stage_kernel(step, length, both, enters, *refs):
-    x_ref, own_ref, own_vectors = refs[:3]
+def stage_kernel(step, length, enters, x_ref, weights_ref, vectors_ref, *refs):
     o_ref = refs[-1]
     plane = lax.axis_index("pp")
     paired = 2 * pair_stages
@@ -105,95 +104,121 @@
     first = jnp.where(in_pair, 2 * mine, 0)
     last = jnp.where(active, jnp.where(in_pair, 2 * mine + 2, 4), first)
     if enters:
-        o_ref[...] = jnp.where(plane < 2, refs[-2][...], x_ref[...])
+        o_ref[...] = jnp.where(plane < 2, refs[0][...], x_ref[...])
     else:
         o_ref[...] = x_ref[...]
     rows = x_ref.shape[0]
-    chans = own_vectors.shape[2]
+    chans = vectors_ref.shape[2]
     at = lax.broadcasted_iota(jnp.int32, (rows // length, length, chans), 1)
 
-    def run(weights, vectors, j):
-        o_ref[...] = section(o_ref[...], weights.at[:, j], vectors[j], at)
-
     def one(j, unused):
-        if not both:
-            run(own_ref, own_vectors, lax.rem(j, 2))
-            return unused
-
-        @pl.when(lax.div(j, 2) == mine)
-        def _():
-            run(own_ref, own_vectors, lax.rem(j, 2))
-
-        @pl.when(lax.div(j, 2) != mine)
-        def _():
-            run(refs[3], refs[4], lax.rem(j, 2))
-
+        o_ref[...] = section(o_ref[...], weights_ref.at[:, j], vectors_ref[j], at)
         return unused
 
     lax.fori_loop(first, last, one, 0)
 
 
-def run_stage(step, length, x, entry, own, other):
-    operands = (x,) + own + (other if other is not None else ()) + (() if entry is None else (entry,))
+def run_stage(step, length, x, entry, weights, vectors):
+    operands = (x, weights, vectors) + (() if entry is None else (entry,))
     rows, width = x.shape
-    chans = own[1].shape[2]
-    sections = 2 if other is None else 4
+    chans = vectors.shape[2]
     spec = pl.BlockSpec(memory_space=pltpu.VMEM)
     return pl.pallas_call(
-        functools.partial(stage_kernel, step, length, other is not None, entry is not None),
+        functools.partial(stage_kernel, step, length, entry is not None),
         out_shape=jax.ShapeDtypeStruct(x.shape, x.dtype),
         in_specs=[spec] * len(operands),
         out_specs=spec,
         compiler_params=pltpu.CompilerParams(vmem_limit_bytes=24 << 20),
         cost_estimate=pl.CostEstimate(
-            flops=4 * sections * rows * width * chans,
-            bytes_accessed=sections * 4 * width * chans,
-            transcendentals=sections * 5 * rows * chans,
+            flops=16 * rows * width * chans,
+            bytes_accessed=16 * width * chans,
+            transcendentals=20 * rows * chans,
         ),
         name="stage",
     )(*operands)
 
 
-def join_kernel(mine_ref, near_ref, o_ref, done):
-    odd = lax.rem(lax.axis_index("pp"), 2)
-    copies = [
-        pltpu.make_async_copy(mine_ref, o_ref.at[:, odd], done.at[0]),
-        pltpu.make_async_copy(near_ref, o_ref.at[:, 1 - odd], done.at[1]),
-    ]
-    for copy in copies:
+def flipped(place, by):
+    if by == 1:
+        return place + 1 - 2 * lax.rem(place, 2)
+    return lax.rem(place + 2, 4) if by == 2 else 3 - place
+
+
+def place_in_plane():
+    part = lax.axis_index("tp")
+    core = lax.rem(part, 2)
+    colour = lax.rem(lax.div(part, 2) + 2 * lax.axis_index("fs"), 4)
+    return colour, core
+
+
+def join_kernel(flips, own, *refs):
+    self_ref, ring_ref, mate_self_ref, mate_ring_ref = refs[:4]
+    o_ref, done = refs[-2:]
+    place = lax.rem(lax.axis_index("pp"), 4)
+    colour, core = place_in_plane()
+    lines = o_ref.shape[2]
+    copies = []
+
+    def put(source, target):
+        copy = pltpu.make_async_copy(source, target, done.at[len(copies)])
         copy.start()
+        copies.append(copy)
+
+    if own:
+        project_ref, back_ref, maps_ref = refs[4:7]
+        depth = project_ref.shape[1]
+        put(project_ref, o_ref.at[:, place, pl.ds(0, depth)])
+        put(maps_ref, o_ref.at[:, place, pl.ds(2 * depth, lines - 2 * depth)])
+        for t in range(o_ref.shape[0]):
+            for h in range(2):
+                put(
+                    back_ref.at[pl.ds(h * depth, depth), pl.ds(t * depth, depth)],
+                    o_ref.at[t, place, pl.ds(depth, depth), pl.ds(h * depth, depth)],
+                )
+    for i, by in enumerate(flips):
+        slot = flipped(place, by)
+        for side, alone, ring in ((core, self_ref, ring_ref), (1 - core, mate_self_ref, mate_ring_ref)):
+            put(alone.at[i], o_ref.at[2 * colour + side, slot])
+            for r, off in enumerate((3, 1, 2)):
+                put(
+                    ring.at[i, pl.ds(r * lines, lines)],
+                    o_ref.at[2 * lax.rem(colour + off, 4) + side, slot],
+                )
     for copy in copies:
         copy.wait()
 
 
-def joined(mine, near):
-    parts, lines, chans = mine.shape
+def joined(flips, pieces, mine=None, stack=None):
+    lines, chans = pieces[0].shape[1:]
+    parts = mine[0].shape[0] if stack is None else stack.shape[0]
+    whole = pl.BlockSpec(memory_space=pl.ANY)
+    here = pl.BlockSpec(memory_space=pltpu.VMEM)
+    count = 8 * len(flips) + (2 + 2 * parts if stack is None else 0)
     return pl.pallas_call(
-        join_kernel,
-        out_shape=jax.ShapeDtypeStruct((parts, 2, lines, chans), mine.dtype),
-        in_specs=[pl.BlockSpec(memory_space=pl.ANY)] * 2,
-        out_specs=pl.BlockSpec(memory_space=pltpu.VMEM),
-        scratch_shapes=[pltpu.SemaphoreType.DMA((2,))],
-        compiler_params=pltpu.CompilerParams(vmem_limit_bytes=12 << 20),
+        functools.partial(join_kernel, flips, stack is None),
+        out_shape=jax.ShapeDtypeStruct((parts, 4, lines, chans), pieces[0].dtype),
+        in_specs=[whole] * 7 if stack is None else [whole] * 4 + [here],
+        out_specs=here,
+        scratch_shapes=[pltpu.SemaphoreType.DMA((count,))],
+        input_output_aliases={} if stack is None else {4: 0},
+        compiler_params=pltpu.CompilerParams(vmem_limit_bytes=24 << 20),
         name="join",
-    )(mine, near)
-
-
-def packed_weights(w_project, w_back, gate_rate, gate_input, parts):
-    width, chans = w_project.shape
-    depth, half, block = width // parts, chans // 2, gate_rate.shape[1]
-    project = w_project.reshape(parts, depth, chans)
-    back = w_back.reshape(2, half, parts, depth).transpose(2, 1, 0, 3).reshape(parts, half, 2 * depth)
+    )(*pieces, *(mine if stack is None else (stack,)))
+
+
+def block_maps(gate_rate, gate_input, parts):
+    block = gate_rate.shape[1]
     place = jnp.arange(parts)[:, None] % (parts // 2) == jnp.arange(parts // 2)[None, :]
     maps = jnp.stack([gate_rate, gate_input], axis=2)[:, :, :, None, :]
     maps = jnp.where(place[:, None, None, :, None], maps, jnp.zeros((), maps.dtype))
-    return jnp.concatenate([project, back, maps.reshape(parts, block, chans)], axis=1)
+    return maps.reshape(parts, block, parts * block)
 
 
 def packed_shard(w_project, w_back, gate_rate, gate_input, parts):
     width, chans = w_project.shape
     depth, half, block = width // parts, chans // 2, gate_rate.shape[1]
-    part = lax.axis_index("tp")
+    colour, core = place_in_plane()
+    part = 2 * colour + core
     project = lax.dynamic_slice_in_dim(w_project, part * depth, depth, 0)
     back = lax.dynamic_slice_in_dim(w_back, part * depth, depth, 1)
     back = jnp.concatenate([back[:half], back[half:]], axis=1)
@@ -223,19 +248,40 @@
     plane = lax.axis_index("pp")
     length, width = tokens_in.shape[2:]
     chans = weight_in.shape[2]
-    odd = plane % 2
     paired = 2 * pair_stages
 
     def moved(x, pairs):
         return lax.ppermute(x, "pp", [(int(a), int(b)) for a, b in pairs])
 
-    def in_order(mine, theirs):
-        return jnp.stack(
-            [jnp.where(odd == 0, mine, theirs), jnp.where(odd == 0, theirs, mine)], axis=0
-        )
-
-    packed = packed_weights(weight_in[0], weight_out[0], gate_rate[0], gate_input[0], parts)
-    shard = packed_shard(weight_in[0], weight_out[0], gate_rate[0], gate_input[0], parts)
+    place = plane % 4
+    near_place = flipped(place, 1)
+
+    def within(x, step_of, members):
+        pairs = [
+            ((z * splits + y) * parts + 2 * i + c, (z * splits + u) * parts + 2 * j + d)
+            for z in members
+            for y in range(splits)
+            for i in range(parts // 2)
+            for c in range(2)
+            for u, j, d in [step_of(y, i, c)]
+        ]
+        return lax.ppermute(x, ("pp", "fs", "tp"), pairs)
+
+    def from_neighbours(x, members):
+        wide, lines = parts // 2, x.shape[1] // 2
+        return [
+            within(x, lambda y, i, c: (y, (i + 1) % wide, c), members),
+            within(x, lambda y, i, c: (y, (i - 1) % wide, c), members),
+            within(x[:, :lines], lambda y, i, c: ((y + 1) % splits, i, c), members),
+            within(x[:, lines:], lambda y, i, c: ((y - 1) % splits, i, c), members),
+        ]
+
+    def from_mate(x, members):
+        return within(x, lambda y, i, c: (y, i, 1 - c), members)
+
+    project = weight_in.reshape(parts, width // parts, chans)
+    maps = block_maps(gate_rate[0], gate_input[0], parts)
+    shard = packed_shard(weight_in[0], weight_out[0], gate_rate[0], gate_input[0], parts)[None]
     swap = [(i, i ^ 1) for i in range(planes)]
     shard_near = moved(shard, swap)
     vector = jnp.concatenate(
@@ -249,37 +295,39 @@
             norm_shift.reshape(-1, chans),
         ],
         axis=0,
-    )
+    )[None]
     vector_near = moved(vector, swap)
-    near = lax.all_gather(shard_near, "tp", axis=0)
-    own_vectors = in_order(vector, vector_near)
-
-    across = [(i, i ^ 2) for i in range(paired, planes)]
-    couple = in_order(shard, shard_near)
-    lines = shard.shape[0] // splits
-    piece = lax.dynamic_slice_in_dim(couple, lax.axis_index("fs") * lines, lines, 1)
-    piece = moved(piece, across)
-    other_vectors = moved(own_vectors, across)
 
     token = tokens_in.reshape(length, width)
     span = planes // group_count
     per = span // 2
     bases = [(g, s) for g in range(group_count) for s in range(2)]
-    collected = jnp.concatenate(
-        [token]
-        + [moved(token, [(span * g + s + 2 * q, span * g + s) for g, s in bases]) for q in range(1, per)],
-        axis=0,
-    )
-    entries = [collected] + [
+    tokens = [
+        moved(token, [(span * g + s + 2 * q, span * g + s) for g, s in bases]) for q in range(1, per)
+    ]
+    shard_near, *tokens = lax.optimization_barrier((shard_near, *tokens))
+    collected = jnp.concatenate([token] + tokens, axis=0)
+    entries = [
         moved(collected, [(span * g + s, s) for s in range(2)]) for g in range(1, group_count)
     ]
 
-    packed, collected, entries[1], piece, other_vectors, near = lax.optimization_barrier(
-        (packed, collected, entries[1], piece, other_vectors, near)
+    everywhere, later = range(planes), range(paired, planes)
+    across = [(i, i ^ 2) for i in later]
+    far = moved(jnp.concatenate([shard, shard_near], axis=0), across)
+    mate_self = from_mate(shard_near, everywhere)
+    ring = jnp.concatenate(from_neighbours(shard_near, everywhere), axis=1)
+    mate_ring = from_mate(ring, everywhere)
+    vectors = jnp.zeros((4,) + vector.shape[1:], vector.dtype)
+    vectors = lax.dynamic_update_slice_in_dim(vectors, vector, place, 0)
+    vectors = lax.dynamic_update_slice_in_dim(vectors, vector_near, near_place, 0)
+    far_vectors = moved(jnp.concatenate([vector, vector_near], axis=0), across)
+    maps, vectors, collected, shard_near, ring, mate_self, mate_ring, *entries = (
+        lax.optimization_barrier(
+            (maps, vectors, collected, shard_near, ring, mate_self, mate_ring, *entries)
+        )
     )
-    entries[0] = collected
-    own = joined(packed, near)
-    other = lax.all_gather(piece, "fs", axis=1, tiled=True)
+    entries = [collected] + entries
+    weights = joined((1,), (shard_near, ring, mate_self, mate_ring), mine=(project, weight_out[0], maps))
 
     stages = stages_of(planes)
     outputs, arrived = [], []
@@ -290,21 +338,39 @@
             x, entry = entry, None
         if step == 1:
             x = lax.optimization_barrier((x, outputs[0]))[0]
-        late = step >= 2 * pair_stages
-        y = run_stage(
-            step, length, x, entry, (own, own_vectors), (other, other_vectors) if late else None
-        )
+        y = run_stage(step, length, x, entry, weights, vectors)
         pairs = [
             (plane_of(i, step - 2 * i, s), plane_of(i + 1, step - 2 * i, s))
             for i in range(stages - 1)
             if 0 <= step - 2 * i < group_count
             for s in range(2)
         ]
-        if step == 2:
-            other = lax.optimization_barrier((other, outputs[1], y))[0]
-            other = lax.all_gather(other, "tp", axis=0)
         arrived.append(moved(y, pairs) if pairs else None)
         outputs.append(y)
+        if step == 3:
+            far, far_vectors, *_ = lax.optimization_barrier((far, far_vectors, y, arrived[2]))
+            far_mate = from_mate(far, later)
+            far_ring = from_neighbours(far, later)
+        if step == 5:
+            far_mate, *far_ring, _, _ = lax.optimization_barrier(
+                (far_mate, *far_ring, y, arrived[4])
+            )
+            far_ring = jnp.concatenate(far_ring, axis=1)
+            far_mate_ring = from_mate(far_ring, later)
+            vectors_late = vectors
+            for by, row in ((2, 0), (3, 1)):
+                vectors_late = lax.dynamic_update_slice_in_dim(
+                    vectors_late, far_vectors[row : row + 1], flipped(place, by), 0
+                )
+        if step == 2 * pair_stages - 2:
+            far_mate_ring, vectors_late, _ = lax.optimization_barrier(
+                (far_mate_ring, vectors_late, y)
+            )
+        if step == 2 * pair_stages - 1:
+            weights = joined(
+                (2, 3), (far, far_ring, far_mate, far_mate_ring), stack=weights
+            )
+            vectors = vectors_late
 
     last = stages - 1
     stay = [plane_of(last, group_count - 1, s) for s in range(2)]

time: 331 us -> 558 us (1.69)
  the two profiles are of different devices: /device:TPU:928 before, /device:TPU:6 now
where the time goes in v2:
time: 558 us; the launch traced here: 548 us
  starting transfers between devices  304 us (54%)
  waiting for transfers between devices  191 us (34%)
  local copies, waits for them, and re-layouts  30.6 us (5%)
  Pallas kernels  18 us (3%)
    ppermute x12, starting transfers between devices, within(): return lax.ppermute(x, ('pp', 'fs', 'tp'), pairs)  194 us
    ppermute x36, waiting for transfers between devices, moved(): return lax.ppermute(x, 'pp', [(int(a), int(b)) for a, b in pairs])  184 us
    ppermute x36, starting transfers between devices, moved(): return lax.ppermute(x, 'pp', [(int(a), int(b)) for a, b in pairs])  109 us
    unnamed x45, local copies, waits for them, and re-layouts  22 us
    pallas_call x22, Pallas kernels, run_stage(): pl.pallas_call(functools.partial(stage_kernel, step, length, entry is not...  11.8 us
  transfers between devices with their start and end apart: 48, of which 12 were waited for; matrix products, arithmetic and copies ran while one was open for 2% of the time, Pallas kernels for 3%

profile of v2, /device:TPU:6, one launch (start us, length us, event | category | flops | bytes accessed | tf_op | source)
XLA Modules:
  0.0 548.4 jit_solution(5009122379932032861)
XLA Ops:
  3.1 3.8 collective-permute-start.1
  10.8 9.3 %collective-permute-done.4 = bf16[8,2048]{1,0:T(8,128)(2,1)S(1)} collective-permute-done((bf16[8,2048]{1,0:T(8,128)(2,1)S(1)}, bf16[8,2048]{1,0:T(8,128)(2,1)S(1)}, u32[]{:S(2)}, u32[]{:S(2)}) %collective-permute-start.4) | collective-permute-done | bytes 32800 | tf_op jit(solution)/shard_map/ppermute | solution.py:254
  22.3 35.1 %collective-permute-start.5 = (bf16[1,576,512]{2,1,0:T(8,128)(2,1)S(1)}, bf16[1,576,512]{2,1,0:T(8,128)(2,1)S(1)}, u32[]{:S(2)}, u32[]{:S(2)}) collective-permute-start(bf16[1,576,512]{2,1,0:T(8,128)(2,1)S(1)} %collective-permute-done.1.refs_0_), channel_id=1, source_target_pairs={{0,2},{1,3},{2,4},{3,5},{4,6},{5,7},{6,0},{7,1},{8,10},{9,11},{10,... | collective-permute-start | bytes 1769480 | tf_op jit(solution)/shard_map/ppermute | solution.py:268
  57.5 30.8 %collective-permute-start.6 = (bf16[1,576,512]{2,1,0:T(8,128)(2,1)S(1)}, bf16[1,576,512]{2,1,0:T(8,128)(2,1)S(1)}, u32[]{:S(2)}, u32[]{:S(2)}) collective-permute-start(bf16[1,576,512]{2,1,0:T(8,128)(2,1)S(1)} %collective-permute-done.1.refs_0_), channel_id=1, source_target_pairs={{0,6},{1,7},{2,0},{3,1},{4,2},{5,3},{6,4},{7,5},{8,14},{9,15},{10,... | collective-permute-start | bytes 1769480 | tf_op jit(solution)/shard_map/ppermute | solution.py:268
  88.3 30.8 %collective-permute-start.7 = (bf16[1,288,512]{2,1,0:T(8,128)(2,1)S(1)}, bf16[1,288,512]{2,1,0:T(8,128)(2,1)S(1)}, u32[]{:S(2)}, u32[]{:S(2)}) collective-permute-start(bf16[1,288,512]{2,1,0:T(8,128)(2,1)S(1)} %get-tuple-element.66), channel_id=1, source_target_pairs={{0,8},{1,9},{2,10},{3,11},{4,12},{5,13},{6,14},{7,15},{8,16},{9,17... | collective-permute-start | bytes 884744 | tf_op jit(solution)/shard_map/ppermute | solution.py:268
  119.2 30.9 %collective-permute-start.8 = (bf16[1,288,512]{2,1,0:T(8,128)(2,1)S(1)}, bf16[1,288,512]{2,1,0:T(8,128)(2,1)S(1)}, u32[]{:S(2)}, u32[]{:S(2)}) collective-permute-start(bf16[1,288,512]{2,1,0:T(8,128)(2,1)S(1)} %get-tuple-element.65), channel_id=1, source_target_pairs={{0,24},{1,25},{2,26},{3,27},{4,28},{5,29},{6,30},{7,31},{8,0},{9,1... | collective-permute-start | bytes 884744 | tf_op jit(solution)/shard_map/ppermute | solution.py:268
  152.6 6.3 %collective-permute-done.8 = bf16[1,288,512]{2,1,0:T(8,128)(2,1)S(1)} collective-permute-done((bf16[1,288,512]{2,1,0:T(8,128)(2,1)S(1)}, bf16[1,288,512]{2,1,0:T(8,128)(2,1)S(1)}, u32[]{:S(2)}, u32[]{:S(2)}) %collective-permute-start.8) | collective-permute-done | bytes 294944 | tf_op jit(solution)/shard_map/ppermute | solution.py:268
  159.6 30.5 %collective-permute-start.10 = (bf16[1,1728,512]{2,1,0:T(8,128)(2,1)}, bf16[1,1728,512]{2,1,0:T(8,128)(2,1)}, u32[]{:S(2)}, u32[]{:S(2)}) collective-permute-start(bf16[1,1728,512]{2,1,0:T(8,128)(2,1)} %constant_dynamic-update-slice_fusion.refs_1_), channel_id=1, source_target_pairs={{0,1},{1,0},{2,3},{3,2},{4,5},{5,4},{6,7},{7,6},{8,9},{9,8},{10,11... | collective-permute-start | bytes 5308424 | tf_op jit(solution)/shard_map/ppermute | solution.py:268
  192.2 3.5 collective-permute-start
  198.1 30.1 %collective-permute-start.9 = (bf16[1,576,512]{2,1,0:T(8,128)(2,1)S(1)}, bf16[1,576,512]{2,1,0:T(8,128)(2,1)S(1)}, u32[]{:S(2)}, u32[]{:S(2)}) collective-permute-start(bf16[1,576,512]{2,1,0:T(8,128)(2,1)S(1)} %collective-permute-done.1.refs_0_), channel_id=1, source_target_pairs={{0,1},{1,0},{2,3},{3,2},{4,5},{5,4},{6,7},{7,6},{8,9},{9,8},{10,11... | collective-permute-start | bytes 1769480 | tf_op jit(solution)/shard_map/ppermute | solution.py:268
  229.4 30.2 %collective-permute-start.18 = (bf16[2,576,512]{2,1,0:T(8,128)(2,1)}, bf16[2,576,512]{2,1,0:T(8,128)(2,1)S(1)}, u32[]{:S(2)}, u32[]{:S(2)}) collective-permute-start(bf16[2,576,512]{2,1,0:T(8,128)(2,1)} %pad_maximum_fusion), channel_id=1, source_target_pairs={{256,320},{288,352},{320,256},{352,288},{384,448},{416,480},{448,3... | collective-permute-start | bytes 3538952 | tf_op jit(solution)/shard_map/ppermute | solution.py:254
  262.3 43.8 %collective-permute-done.13.refs_0_ = bf16[32,2048]{1,0:T(8,128)(2,1)S(1)} collective-permute-done((bf16[32,2048]{1,0:T(8,128)(2,1)S(1)}, bf16[32,2048]{1,0:T(8,128)(2,1)S(1)}, u32[]{:S(2)}, u32[]{:S(2)}) %collective-permute-start.13) | collective-permute-done | bytes 131104 | tf_op jit(solution)/shard_map/ppermute | solution.py:254
  309.0 4.6 collective-permute-done.12.refs_0_
  313.6 8.1 %collective-permute-done.11.x_ref = bf16[32,2048]{1,0:T(8,128)(2,1)S(1)} collective-permute-done((bf16[32,2048]{1,0:T(8,128)(2,1)S(1)}, bf16[32,2048]{1,0:T(8,128)(2,1)S(1)}, u32[]{:S(2)}, u32[]{:S(2)}) %collective-permute-start.11) | collective-permute-done | bytes 131104 | tf_op jit(solution)/shard_map/ppermute | solution.py:254
  324.9 2.8 join.2.weights_ref.refs_4_
  340.6 5.3 collective-permute-start.15
  346.7 34.2 %collective-permute-start.19 = (f32[2,16,512]{2,1,0:T(8,128)S(1)}, f32[2,16,512]{2,1,0:T(8,128)S(1)}, u32[]{:S(2)}, u32[]{:S(2)}) collective-permute-start(f32[2,16,512]{2,1,0:T(8,128)S(1)} %pad_maximum_fusion.3), channel_id=1, source_target_pairs={{256,320},{288,352},{320,256},{352,288},{384,448},{416,480},{448,3... | collective-permute-start | bytes 196616 | tf_op jit(solution)/shard_map/ppermute | solution.py:254
  380.9 2.8 stage.27
  386.0 4.7 collective-permute-start.26
  402.4 6.4 %copy-done.1 = bf16[8,4,576,512]{3,2,1,0:T(8,128)(2,1)S(1)} copy-done((bf16[8,4,576,512]{3,2,1,0:T(8,128)(2,1)S(1)}, bf16[8,4,576,512]{3,2,1,0:T(8,128)(2,1)}, u32[]{:S(2)}) %copy-start.1) | copy-done | bytes 18874392
  410.4 3.4 join.3.weights_ref
  425.3 6.4 %copy-done.3 = bf16[8,4,576,512]{3,2,1,0:T(8,128)(2,1)S(1)} copy-done((bf16[8,4,576,512]{3,2,1,0:T(8,128)(2,1)S(1)}, bf16[8,4,576,512]{3,2,1,0:T(8,128)(2,1)}, u32[]{:S(2)}) %copy-start.3) | copy-done | bytes 18874392
  431.7 105.7 %collective-permute-done.33 = bf16[32,2048]{1,0:T(8,128)(2,1)S(1)} collective-permute-done((bf16[32,2048]{1,0:T(8,128)(2,1)S(1)}, bf16[32,2048]{1,0:T(8,128)(2,1)S(1)}, u32[]{:S(2)}, u32[]{:S(2)}) %collective-permute-start.33) | collective-permute-done | bytes 131104 | tf_op jit(solution)/shard_map/ppermute | solution.py:254
  541.4 5.0 collective-permute-done.46
  (181 shorter events, 72.5 us)
Async XLA Ops:
  3.1 19.3 %collective-permute-start.1 = (bf16[1,576,512]{2,1,0:T(8,128)(2,1)S(1)}, bf16[1,576,512]{2,1,0:T(8,128)(2,1)S(1)}, u32[]{:S(2)}, u32[]{:S(2)}) collective-permute-start(bf16[1,576,512]{2,1,0:T(8,128)(2,1)S(1)} %maximum_bitcast_fusion), channel_id=1, source_target_pairs={{0,32},{32,0},{64,96},{96,64},{128,160},{160,128},{192,224},{224,1... | collective-permute-start | bytes 1769480 | tf_op jit(solution)/shard_map/ppermute | solution.py:254
  6.9 13.2 %collective-permute-start.4 = (bf16[8,2048]{1,0:T(8,128)(2,1)S(1)}, bf16[8,2048]{1,0:T(8,128)(2,1)S(1)}, u32[]{:S(2)}, u32[]{:S(2)}) collective-permute-start(bf16[8,2048]{1,0:T(8,128)(2,1)S(1)} %bitcast.28), channel_id=1, source_target_pairs={{192,0},{224,32},{448,256},{480,288},{704,512},{736,544},{960,768}... | collective-permute-start | bytes 98312 | tf_op jit(solution)/shard_map/ppermute | solution.py:254
  8.2 11.9 %collective-permute-start.3 = (bf16[8,2048]{1,0:T(8,128)(2,1)S(1)}, bf16[8,2048]{1,0:T(8,128)(2,1)S(1)}, u32[]{:S(2)}, u32[]{:S(2)}) collective-permute-start(bf16[8,2048]{1,0:T(8,128)(2,1)S(1)} %bitcast.29), channel_id=1, source_target_pairs={{128,0},{160,32},{384,256},{416,288},{640,512},{672,544},{896,768}... | collective-permute-start | bytes 98312 | tf_op jit(solution)/shard_map/ppermute | solution.py:254
  9.5 10.6 %collective-permute-start.2 = (bf16[8,2048]{1,0:T(8,128)(2,1)S(1)}, bf16[8,2048]{1,0:T(8,128)(2,1)S(1)}, u32[]{:S(2)}, u32[]{:S(2)}) collective-permute-start(bf16[8,2048]{1,0:T(8,128)(2,1)S(1)} %bitcast.30), channel_id=1, source_target_pairs={{64,0},{96,32},{320,256},{352,288},{576,512},{608,544},{832,768},{... | collective-permute-start | bytes 98312 | tf_op jit(solution)/shard_map/ppermute | solution.py:254
  22.3 127.8 %collective-permute-start.5 = (bf16[1,576,512]{2,1,0:T(8,128)(2,1)S(1)}, bf16[1,576,512]{2,1,0:T(8,128)(2,1)S(1)}, u32[]{:S(2)}, u32[]{:S(2)}) collective-permute-start(bf16[1,576,512]{2,1,0:T(8,128)(2,1)S(1)} %collective-permute-done.1.refs_0_), channel_id=1, source_target_pairs={{0,2},{1,3},{2,4},{3,5},{4,6},{5,7},{6,0},{7,1},{8,10},{9,11},{10,... | collective-permute-start | bytes 1769480 | tf_op jit(solution)/shard_map/ppermute | solution.py:268
  57.5 93.5 %collective-permute-start.6 = (bf16[1,576,512]{2,1,0:T(8,128)(2,1)S(1)}, bf16[1,576,512]{2,1,0:T(8,128)(2,1)S(1)}, u32[]{:S(2)}, u32[]{:S(2)}) collective-permute-start(bf16[1,576,512]{2,1,0:T(8,128)(2,1)S(1)} %collective-permute-done.1.refs_0_), channel_id=1, source_target_pairs={{0,6},{1,7},{2,0},{3,1},{4,2},{5,3},{6,4},{7,5},{8,14},{9,15},{10,... | collective-permute-start | bytes 1769480 | tf_op jit(solution)/shard_map/ppermute | solution.py:268
  88.3 63.5 %collective-permute-start.7 = (bf16[1,288,512]{2,1,0:T(8,128)(2,1)S(1)}, bf16[1,288,512]{2,1,0:T(8,128)(2,1)S(1)}, u32[]{:S(2)}, u32[]{:S(2)}) collective-permute-start(bf16[1,288,512]{2,1,0:T(8,128)(2,1)S(1)} %get-tuple-element.66), channel_id=1, source_target_pairs={{0,8},{1,9},{2,10},{3,11},{4,12},{5,13},{6,14},{7,15},{8,16},{9,17... | collective-permute-start | bytes 884744 | tf_op jit(solution)/shard_map/ppermute | solution.py:268
  119.2 39.6 %collective-permute-start.8 = (bf16[1,288,512]{2,1,0:T(8,128)(2,1)S(1)}, bf16[1,288,512]{2,1,0:T(8,128)(2,1)S(1)}, u32[]{:S(2)}, u32[]{:S(2)}) collective-permute-start(bf16[1,288,512]{2,1,0:T(8,128)(2,1)S(1)} %get-tuple-element.65), channel_id=1, source_target_pairs={{0,24},{1,25},{2,26},{3,27},{4,28},{5,29},{6,30},{7,31},{8,0},{9,1... | collective-permute-start | bytes 884744 | tf_op jit(solution)/shard_map/ppermute | solution.py:268
  159.6 162.1 %collective-permute-start.10 = (bf16[1,1728,512]{2,1,0:T(8,128)(2,1)}, bf16[1,1728,512]{2,1,0:T(8,128)(2,1)}, u32[]{:S(2)}, u32[]{:S(2)}) collective-permute-start(bf16[1,1728,512]{2,1,0:T(8,128)(2,1)} %constant_dynamic-update-slice_fusion.refs_1_), channel_id=1, source_target_pairs={{0,1},{1,0},{2,3},{3,2},{4,5},{5,4},{6,7},{7,6},{8,9},{9,8},{10,11... | collective-permute-start | bytes 5308424 | tf_op jit(solution)/shard_map/ppermute | solution.py:268
  192.2 68.8 %collective-permute-start = (f32[1,16,512]{2,1,0:T(8,128)S(1)}, f32[1,16,512]{2,1,0:T(8,128)}, u32[]{:S(2)}, u32[]{:S(2)}) collective-permute-start(f32[1,16,512]{2,1,0:T(8,128)S(1)} %bitcast.24), channel_id=1, source_target_pairs={{0,32},{32,0},{64,96},{96,64},{128,160},{160,128},{192,224},{224,1... | collective-permute-start | bytes 98312 | tf_op jit(solution)/shard_map/ppermute | solution.py:254
  198.1 123.6 %collective-permute-start.9 = (bf16[1,576,512]{2,1,0:T(8,128)(2,1)S(1)}, bf16[1,576,512]{2,1,0:T(8,128)(2,1)S(1)}, u32[]{:S(2)}, u32[]{:S(2)}) collective-permute-start(bf16[1,576,512]{2,1,0:T(8,128)(2,1)S(1)} %collective-permute-done.1.refs_0_), channel_id=1, source_target_pairs={{0,1},{1,0},{2,3},{3,2},{4,5},{5,4},{6,7},{7,6},{8,9},{9,8},{10,11... | collective-permute-start | bytes 1769480 | tf_op jit(solution)/shard_map/ppermute | solution.py:268
  229.4 154.3 %collective-permute-start.18 = (bf16[2,576,512]{2,1,0:T(8,128)(2,1)}, bf16[2,576,512]{2,1,0:T(8,128)(2,1)S(1)}, u32[]{:S(2)}, u32[]{:S(2)}) collective-permute-start(bf16[2,576,512]{2,1,0:T(8,128)(2,1)} %pad_maximum_fusion), channel_id=1, source_target_pairs={{256,320},{288,352},{320,256},{352,288},{384,448},{416,480},{448,3... | collective-permute-start | bytes 3538952 | tf_op jit(solution)/shard_map/ppermute | solution.py:254
  259.6 46.5 %collective-permute-start.13 = (bf16[32,2048]{1,0:T(8,128)(2,1)S(1)}, bf16[32,2048]{1,0:T(8,128)(2,1)S(1)}, u32[]{:S(2)}, u32[]{:S(2)}) collective-permute-start(bf16[32,2048]{1,0:T(8,128)(2,1)S(1)} %pad_maximum_fusion.2.x_ref), channel_id=1, source_target_pairs={{768,0},{800,32},{769,1},{801,33},{770,2},{802,34},{771,3},{803,35... | collective-permute-start | bytes 393224 | tf_op jit(solution)/shard_map/ppermute | solution.py:254
  261.0 52.6 %collective-permute-start.12 = (bf16[32,2048]{1,0:T(8,128)(2,1)S(1)}, bf16[32,2048]{1,0:T(8,128)(2,1)S(1)}, u32[]{:S(2)}, u32[]{:S(2)}) collective-permute-start(bf16[32,2048]{1,0:T(8,128)(2,1)S(1)} %pad_maximum_fusion.2.x_ref), channel_id=1, source_target_pairs={{512,0},{544,32},{513,1},{545,33},{514,2},{546,34},{515,3},{547,35... | collective-permute-start | bytes 393224 | tf_op jit(solution)/shard_map/ppermute | solution.py:254
  306.1 15.6 %collective-permute-start.11 = (bf16[32,2048]{1,0:T(8,128)(2,1)S(1)}, bf16[32,2048]{1,0:T(8,128)(2,1)S(1)}, u32[]{:S(2)}, u32[]{:S(2)}) collective-permute-start(bf16[32,2048]{1,0:T(8,128)(2,1)S(1)} %pad_maximum_fusion.2.x_ref), channel_id=1, source_target_pairs={{256,0},{288,32},{257,1},{289,33},{258,2},{290,34},{259,3},{291,35... | collective-permute-start | bytes 393224 | tf_op jit(solution)/shard_map/ppermute | solution.py:254
  334.6 46.3 %collective-permute-start.20 = (bf16[32,2048]{1,0:T(8,128)(2,1)S(1)}, bf16[32,2048]{1,0:T(8,128)(2,1)S(1)}, u32[]{:S(2)}, u32[]{:S(2)}) collective-permute-start(bf16[32,2048]{1,0:T(8,128)(2,1)S(1)} %stage.26), channel_id=1, source_target_pairs={{0,64},{32,96},{1,65},{33,97},{2,66},{34,98},{3,67},{35,99},{4,68}... | collective-permute-start | bytes 393224 | tf_op jit(solution)/shard_map/ppermute | solution.py:254
  340.6 43.1 %collective-permute-start.15 = (bf16[32,2048]{1,0:T(8,128)(2,1)S(1)}, bf16[32,2048]{1,0:T(8,128)(2,1)S(1)}, u32[]{:S(2)}, u32[]{:S(2)}) collective-permute-start(bf16[32,2048]{1,0:T(8,128)(2,1)S(1)} %stage.23), channel_id=1, source_target_pairs={{0,64},{32,96},{64,128},{96,160},{1,65},{33,97},{65,129},{97,161},... | collective-permute-start | bytes 393224 | tf_op jit(solution)/shard_map/ppermute | solution.py:254
  346.7 37.0 %collective-permute-start.19 = (f32[2,16,512]{2,1,0:T(8,128)S(1)}, f32[2,16,512]{2,1,0:T(8,128)S(1)}, u32[]{:S(2)}, u32[]{:S(2)}) collective-permute-start(f32[2,16,512]{2,1,0:T(8,128)S(1)} %pad_maximum_fusion.3), channel_id=1, source_target_pairs={{256,320},{288,352},{320,256},{352,288},{384,448},{416,480},{448,3... | collective-permute-start | bytes 196616 | tf_op jit(solution)/shard_map/ppermute | solution.py:254
  383.7 11.5 %collective-permute-start.23 = (bf16[2,576,512]{2,1,0:T(8,128)(2,1)S(1)}, bf16[2,576,512]{2,1,0:T(8,128)(2,1)S(1)}, u32[]{:S(2)}, u32[]{:S(2)}) collective-permute-start(bf16[2,576,512]{2,1,0:T(8,128)(2,1)S(1)} %collective-permute-done.18.refs_0_), channel_id=1, source_target_pairs={{256,262},{257,263},{258,256},{259,257},{260,258},{261,259},{262,2... | collective-permute-start | bytes 3538952 | tf_op jit(solution)/shard_map/ppermute | solution.py:268
  384.5 10.8 %collective-permute-start.22 = (bf16[2,576,512]{2,1,0:T(8,128)(2,1)S(1)}, bf16[2,576,512]{2,1,0:T(8,128)(2,1)S(1)}, u32[]{:S(2)}, u32[]{:S(2)}) collective-permute-start(bf16[2,576,512]{2,1,0:T(8,128)(2,1)S(1)} %collective-permute-done.18.refs_0_), channel_id=1, source_target_pairs={{256,258},{257,259},{258,260},{259,261},{260,262},{261,263},{262,2... | collective-permute-start | bytes 3538952 | tf_op jit(solution)/shard_map/ppermute | solution.py:268
  399.2 11.2 %collective-permute-start.27 = (bf16[2,1728,512]{2,1,0:T(8,128)(2,1)}, bf16[2,1728,512]{2,1,0:T(8,128)(2,1)}, u32[]{:S(2)}, u32[]{:S(2)}) collective-permute-start(bf16[2,1728,512]{2,1,0:T(8,128)(2,1)} %constant_dynamic-update-slice_fusion.4.refs_1_), channel_id=1, source_target_pairs={{256,257},{257,256},{258,259},{259,258},{260,261},{261,260},{262,2... | collective-permute-start | bytes 10616840 | tf_op jit(solution)/shard_map/ppermute | solution.py:268
  421.8 115.6 %collective-permute-start.33 = (bf16[32,2048]{1,0:T(8,128)(2,1)S(1)}, bf16[32,2048]{1,0:T(8,128)(2,1)S(1)}, u32[]{:S(2)}, u32[]{:S(2)}) collective-permute-start(bf16[32,2048]{1,0:T(8,128)(2,1)S(1)} %stage.34), channel_id=1, source_target_pairs={{896,0},{928,32},{897,1},{929,33},{898,2},{930,34},{899,3},{931,35... | collective-permute-start | bytes 393224 | tf_op jit(solution)/shard_map/ppermute | solution.py:254
  423.8 113.6 %collective-permute-start.41 = (bf16[32,2048]{1,0:T(8,128)(2,1)S(1)}, bf16[32,2048]{1,0:T(8,128)(2,1)S(1)}, u32[]{:S(2)}, u32[]{:S(2)}) collective-permute-start(bf16[32,2048]{1,0:T(8,128)(2,1)S(1)} %stage.41), channel_id=1, source_target_pairs={{960,256},{992,288},{961,257},{993,289},{962,258},{994,290},{963,2... | collective-permute-start | bytes 393224 | tf_op jit(solution)/shard_map/ppermute | solution.py:254
  424.6 112.8 %collective-permute-start.43 = (bf16[32,2048]{1,0:T(8,128)(2,1)S(1)}, bf16[32,2048]{1,0:T(8,128)(2,1)S(1)}, u32[]{:S(2)}, u32[]{:S(2)}) collective-permute-start(bf16[32,2048]{1,0:T(8,128)(2,1)S(1)} %stage.42), channel_id=1, source_target_pairs={{896,512},{928,544},{897,513},{929,545},{898,514},{930,546},{899,5... | collective-permute-start | bytes 393224 | tf_op jit(solution)/shard_map/ppermute | solution.py:254
  (43 other events, 930.7 us)
